TPU v7x, 256 devices: a whole 4x4x8 slice. The times are simulated.
256 devices in a mesh: kv: 32 (over z, y), tp: 8 (over x, core).
Axes of the slice: x: 4, y: 4, z: 8, core: 2. Of those that a mesh axis runs over, the one named last changes fastest.
Arguments:
- tokens: bfloat16 [16, 4, 4096], P(None, None, 'kv'), may hold values from -20 to 20
- mix_gain: float32 [4096], P('kv'), may hold values from 0.1 to 1.9
- w_query: bfloat16 [4096, 2048], P('kv', 'tp'), may hold values from -0.09375 to 0.09375
- w_key: bfloat16 [4096, 2048], P('kv', 'tp'), may hold values from -0.09375 to 0.09375
- w_value: bfloat16 [4096, 2048], P('kv', 'tp'), may hold values from -0.09375 to 0.09375
- w_forget: bfloat16 [4096, 16], replicated, may hold values from -0.09375 to 0.09375
- forget_bias: float32 [16], P('tp'), may hold values from -1 to 3
- key_cache: bfloat16 [16, 16384, 2048], P(None, 'kv', 'tp'), may hold values from -6 to 6
- value_cache: bfloat16 [16, 16384, 2048], P(None, 'kv', 'tp'), may hold values from -6 to 6
- cum_gate: float32 [16, 16, 16384], P(None, 'tp', 'kv'), may hold values from -2236.08 to 0, as said below
- lengths: int32 [16], replicated, may hold values from 1 to 16384, 65524 in all
- w_out: bfloat16 [2048, 4096], P('tp', 'kv'), may hold values from -0.125 to 0.125
- mlp_gain: float32 [4096], P('kv'), may hold values from 0.1 to 1.9
- w_gate: bfloat16 [4096, 11264], P('kv', 'tp'), may hold values from -0.09375 to 0.09375
- w_up: bfloat16 [4096, 11264], P('kv', 'tp'), may hold values from -0.09375 to 0.09375
- w_down: bfloat16 [11264, 4096], P('tp', 'kv'), may hold values from -0.0546875 to 0.0546875
Outputs:
- result: bfloat16 [16, 4, 4096], P(None, None, 'kv')
Inputs may be any that keep to these rules, and one draw needn't show every extreme that they name: `cum_gate`: never rising along positions. `lengths`: one sequence fills all 16384 positions.
All inputs are finite; a program needn't handle non-finite values.
Results may differ from a plain program's by a relative error of at most 0.02.
Values may be sent and summed in bfloat16 or wider, within the bound.
A program may use at most 64 MiB of HBM per device.

v0:
```python
import jax
import jax.numpy as jnp
from jax import lax
from jax.sharding import Mesh
from jax.sharding import PartitionSpec as P

D = 4096
KV = ("kv_0", "kv_1")


EPSILON = 1e-06
NEG_FILL = -1e30


def in_one(arrays, axis):
    flat, at, outs = (jnp.concatenate([a.reshape(-1) for a in arrays]), 0, [])
    running = lax.psum(flat, axis)
    for a in arrays:
        outs.append(running[at : at + a.size].reshape(a.shape))
        at += a.size
    return tuple(outs)


def all_in_one(array, axis):
    leaves = jax.tree.leaves(array)
    turns = sorted(range(len(leaves)), key=lambda k: -leaves[k].size)
    width = (1, *leaves[turns[0]].shape)[-1]
    lines = [
        jnp.pad(leaves[k].reshape(-1), (0, -leaves[k].size % width)).reshape(-1, width)
        for k in turns
    ]
    both, at, found = (lax.all_gather(jnp.concatenate(lines), axis), 0, {})
    for k, line in zip(turns, lines):
        share = both[:, at : at + len(line)].reshape(len(both), -1)
        found[k] = share[:, : leaves[k].size].reshape(-1, *leaves[k].shape)
        at += len(line)
    numbers = iter(range(len(leaves)))
    return jax.tree.map(lambda _: found[next(numbers)], array)


def merged_by_axis(array, axes, combine):
    for axis in axes:
        pieces = all_in_one(array, axis)
        array = jax.tree.map(lambda part: part[0], pieces)
        for k in range(1, lax.axis_size(axis)):
            array = combine(array, jax.tree.map(lambda part: part[k], pieces))
    return array


def sent_to_all(array, axis):
    peers = lax.axis_size(axis)
    return lax.all_to_all(
        jnp.broadcast_to(array[None], (peers, *array.shape)), axis, 0, 0, tiled=True
    )


def of_everyone(array, axis):
    return sent_to_all(array, axis).astype(jnp.float32).sum(axis=0)


def over_copies(array, axis):
    everything = sent_to_all(array, axis)
    return jnp.sum(everything, axis=0)


def cut_along(array, dim, peers):
    shape = array.shape
    tiles = array.reshape(*shape[:dim], peers, shape[dim] // peers, *shape[dim + 1 :])
    return jnp.moveaxis(tiles, dim, 0)


def sum_at_owner(array, axis, dim):
    tiles = cut_along(array, dim, lax.axis_size(axis))
    arrived = lax.all_to_all(tiles, axis, split_axis=0, concat_axis=0, tiled=True)
    return arrived.astype(jnp.float32).sum(axis=0)


def sent_together(arrays, axis, dim, along):
    ends, at = ([], 0)
    for a in arrays[:-1]:
        at += a.shape[along]
        ends.append(at)
    both = jnp.concatenate(arrays, axis=along)
    return tuple(jnp.split(sum_at_owner(both, axis, dim), ends, axis=along))


def joined_along(tiles, dim):
    tiles = jnp.moveaxis(tiles, 0, dim)
    shape = tiles.shape
    return tiles.reshape(*shape[:dim], shape[dim] * shape[dim + 1], *shape[dim + 2 :])


def collect(array, axis, dim):
    tiles = sent_to_all(array, axis)
    return joined_along(tiles, dim)


def on_device(
    tokens,
    mix_gain,
    w_query,
    w_key,
    w_value,
    w_forget,
    forget_bias,
    key_cache,
    value_cache,
    cum_gate,
    lengths,
    w_out,
    mlp_gain,
    w_gate,
    w_up,
    w_down,
):
    seq_count, new_count, local_width = tokens.shape
    row_count = seq_count * new_count
    heads_dev = forget_bias.shape[0]
    head_width = w_query.shape[1] // heads_dev
    pos_dev = key_cache.shape[1]
    kv_index = lax.axis_index(KV)
    tp_index = lax.axis_index("tp")
    inputs = tokens.reshape(row_count, local_width).astype(jnp.float32)
    scaled = (inputs * mix_gain).astype(jnp.bfloat16)
    forget_rows = lax.dynamic_slice_in_dim(w_forget, kv_index * local_width, local_width, 0)
    forget_cols = lax.dynamic_slice_in_dim(forget_rows, tp_index * heads_dev, heads_dev, 1)
    query_part = jnp.dot(scaled, w_query, preferred_element_type=jnp.float32)
    key_part = jnp.dot(scaled, w_key, preferred_element_type=jnp.float32)
    value_part = jnp.dot(scaled, w_value, preferred_element_type=jnp.float32)
    forget_part = jnp.dot(scaled, forget_cols, preferred_element_type=jnp.float32)
    squares = jnp.sum(inputs * inputs, axis=1)
    query_sum, key_sum, value_sum, forget_sum, square_sum = tuple(
        (
            part.astype(jnp.float32)
            for part in in_one(
                (
                    query_part.astype(jnp.bfloat16),
                    key_part.astype(jnp.bfloat16),
                    value_part.astype(jnp.bfloat16),
                    forget_part.astype(jnp.bfloat16),
                    squares.astype(jnp.bfloat16),
                ),
                KV,
            )
        )
    )
    inv_norm = lax.rsqrt(square_sum / D + EPSILON)[:, None]
    head_shape = (seq_count, new_count, heads_dev, head_width)
    query = (inv_norm * query_sum).astype(jnp.bfloat16).reshape(head_shape)
    key_new = (inv_norm * key_sum).astype(jnp.bfloat16).reshape(head_shape)
    value_new = (inv_norm * value_sum).astype(jnp.bfloat16).reshape(head_shape)
    log_forget = jax.nn.log_sigmoid(inv_norm * forget_sum + forget_bias).reshape(
        seq_count, new_count, heads_dev
    )
    score_scale = head_width ** (-0.5)
    positions = kv_index * pos_dev + jnp.arange(pos_dev, dtype=jnp.int32)
    live_rows = positions[None, :] < lengths[:, None]
    live_mask = live_rows[:, None, None, :]
    cached_keys = key_cache.reshape(seq_count, pos_dev, heads_dev, head_width)
    cached_values = value_cache.reshape(seq_count, pos_dev, heads_dev, head_width)
    scores = jnp.einsum("bthd,bphd->bthp", query, cached_keys, preferred_element_type=jnp.float32)
    scores = scores * score_scale - cum_gate[:, None]
    scores = jnp.where(live_mask, scores, NEG_FILL)
    block_peak = jnp.max(scores, axis=3)
    weights = jnp.where(live_mask, jnp.exp(scores - block_peak[..., None]), 0.0)
    block_total = jnp.sum(weights, axis=3)
    block_sum = jnp.einsum(
        "bthp,bphd->bthd",
        weights.astype(jnp.bfloat16),
        cached_values,
        preferred_element_type=jnp.float32,
    )
    last_hit = positions[None, :] == (lengths - 1)[:, None]
    last_piece = jnp.sum(jnp.where(last_hit[:, None, :], cum_gate, 0.0), axis=2)

    def combine(first, second):
        peak_both = jnp.maximum(first[0], second[0])
        first_factor = jnp.exp(first[0] - peak_both)
        second_factor = jnp.exp(second[0] - peak_both)
        return (
            peak_both,
            first[1] * first_factor + second[1] * second_factor,
            first[2] * first_factor[..., None] + second[2] * second_factor[..., None],
            first[3] + second[3],
        )

    past_peak, past_total, past_sum, last_cum = merged_by_axis(
        (block_peak, block_total, block_sum, last_piece), KV, combine
    )
    key_cum = last_cum[:, None, :] + jnp.cumsum(log_forget, axis=1)
    own_scores = (
        jnp.einsum("bthd,bshd->bths", query, key_new, preferred_element_type=jnp.float32)
        * score_scale
    )
    own_scores = own_scores - jnp.transpose(key_cum, (0, 2, 1))[:, None]
    causal = (jnp.arange(new_count)[:, None] >= jnp.arange(new_count)[None, :])[None, :, None, :]
    own_scores = jnp.where(causal, own_scores, NEG_FILL)
    peak_score = jnp.maximum(past_peak, jnp.max(own_scores, axis=3))
    past_factor = jnp.exp(past_peak - peak_score)
    own_weights = jnp.where(causal, jnp.exp(own_scores - peak_score[..., None]), 0.0)
    numerator = past_sum * past_factor[..., None] + jnp.einsum(
        "bths,bshd->bthd",
        own_weights.astype(jnp.bfloat16),
        value_new,
        preferred_element_type=jnp.float32,
    )
    denominator = past_total * past_factor + jnp.sum(own_weights, axis=3)
    attended = (
        (numerator / denominator[..., None])
        .astype(jnp.bfloat16)
        .reshape(row_count, heads_dev * head_width)
    )
    attn_out = of_everyone(
        jnp.dot(attended, w_out, preferred_element_type=jnp.float32).astype(jnp.bfloat16), "tp"
    ).astype(jnp.float32)
    middle = (inputs + attn_out).astype(jnp.bfloat16)
    middle_wide = middle.astype(jnp.float32)
    squares2 = jnp.sum(middle_wide * middle_wide, axis=1)
    scaled2 = (middle_wide * mlp_gain).astype(jnp.bfloat16)
    gate_part = jnp.dot(scaled2, w_gate, preferred_element_type=jnp.float32)
    up_part = jnp.dot(scaled2, w_up, preferred_element_type=jnp.float32)
    kv_count = lax.axis_size(KV)
    share_rows = (row_count + kv_count - 1) // kv_count
    square_sum2 = over_copies(squares2, KV)
    gate_share, up_share = sent_together(
        (gate_part.astype(jnp.bfloat16), up_part.astype(jnp.bfloat16)), KV, 0, 1
    )
    share_squares = lax.dynamic_slice_in_dim(square_sum2, kv_index * share_rows, share_rows, 0)
    inv_norm2 = lax.rsqrt(share_squares / D + EPSILON)[:, None]
    hidden_share = (jax.nn.silu(inv_norm2 * gate_share) * (inv_norm2 * up_share)).astype(
        jnp.bfloat16
    )
    down_full = jnp.dot(collect(hidden_share, KV, 0), w_down, preferred_element_type=jnp.float32)
    mixed = of_everyone(down_full.astype(jnp.bfloat16), "tp").astype(jnp.float32)
    return (middle_wide + mixed).astype(jnp.bfloat16).reshape(seq_count, new_count, local_width)


def solution(mesh):
    split = Mesh(mesh.devices.reshape(8, 4, mesh.shape["tp"]), ("kv_0", "kv_1", "tp"))
    return jax.shard_map(
        on_device,
        mesh=split,
        in_specs=(
            P(None, None, KV),
            P(KV),
            P(KV, "tp"),
            P(KV, "tp"),
            P(KV, "tp"),
            P(),
            P("tp"),
            P(None, KV, "tp"),
            P(None, KV, "tp"),
            P(None, "tp", KV),
            P(),
            P("tp", KV),
            P(KV),
            P(KV, "tp"),
            P(KV, "tp"),
            P("tp", KV),
        ),
        out_specs=P(None, None, KV),
        check_vma=False,
    )
```

profile of v0, /device:TPU:1, one launch (start us, length us, event | category | flops | bytes accessed | tf_op | source)
XLA Modules:
  0.0 287.4 jit_solution(13230378988156012620)
XLA Ops:
  6.5 0.9 multiply_reduce_fusion
  7.5 0.7 multiply_convert_fusion.1
  8.3 0.9 convolution_convert_fusion.7
  9.2 0.1 copy.145
  9.3 0.2 reshape.1196
  9.4 1.0 fusion.23
  10.4 1.0 fusion.22
  11.5 1.0 fusion.21
  12.5 0.2 dynamic-update-slice.3
  12.7 0.2 dynamic-update-slice.4
  12.9 0.6 copy-done.4
  13.6 0.7 broadcast_add_fusion
  14.3 0.7 broadcast_compare_fusion.1
  15.0 1.0 select_reduce_fusion
  16.1 139.1 %all-reduce.4.cloned.1.call-done = bf16[49344]{0:T(1024)(128)(2,1)} async-done(((bf16[49344]{0:T(1024)(128)(2,1)}), bf16[49344]{0:T(1024)(128)(2,1)}) %all-reduce.4.cloned.1.call-update) | async-done | bytes 98704 | tf_op jit(solution)/shard_map/psum | solution.py:17
  155.2 0.7 fusion.103
  156.0 0.8 fusion.122
  157.0 3.5 %fusion.123 = (f32[16,4,2]{1,2,0:T(2,128)S(1)}, f32[16,4,2,512]{3,1,2,0:T(4,128)S(1)}) fusion(f32[16,2,512]{2,1,0:T(2,128)} %param.25, bf16[16,4,2,128]{3,0,2,1:T(8,128)(2,1)S(1)} %get-tuple-element.61, pred[16,512]{1,0:T(8,128)(4,1)S(1)} %get-tuple-element.62, bf16[16,512,256]{2,1,0:T(8,128)(2,1)} %param.23), kind=kOutput, calls=%fused_computation.233 | convolution fusion | flops 17039232 | bytes 4563456 | tf_op jit(solution)/shard_map/bthd,bphd->bthp/dot_general | solution.py:161
  160.5 0.2 copy.152
  160.7 0.3 fusion.24
  161.0 2.9 %fusion.18 = f32[16,4,2,128]{3,1,2,0:T(4,128)S(1)} fusion(f32[16,4,2,512]{3,1,2,0:T(4,128)S(1)} %get-tuple-element.65, f32[16,4,2]{1,2,0:T(2,128)S(1)} %get-tuple-element.64, pred[16,512]{1,0:T(8,128)(4,1)S(1)} %get-tuple-element.62, bf16[16,512,256]{2,1,0:T(8,128)(2,1)} %param.24), kind=kOutput, calls=%fused_computation.12 | convolution fusion | flops 16973824 | bytes 4530688 | tf_op jit(solution)/shard_map/bthp,bphd->bthd/dot_general | solution.py:167
  164.0 0.1 reshape.1200
  164.2 0.2 copy.153
  164.4 0.1 reshape.1201
  164.5 19.4 %all-gather.2 = f32[8,131,128]{2,1,0:T(8,128)S(1)} all-gather(f32[1,131,128]{2,1,0:T(8,128)S(1)} %maximum_bitcast_fusion), channel_id=2, replica_groups=mesh['kv_0'=8,'kv_1'=4,'tp'=8] {'kv_0'}, dimensions={0}, use_global_device_ids=true | all-gather | bytes 603648 | tf_op jit(solution)/shard_map/all_gather | solution.py:32
  184.1 0.3 fusion.31
  184.4 9.9 %all-gather.3 = f32[4,131,128]{2,1,0:T(8,128)S(1)} all-gather(f32[1,131,128]{2,1,0:T(8,128)S(1)} %maximum_bitcast_fusion.1), channel_id=3, replica_groups=mesh['kv_0'=8,'kv_1'=4,'tp'=8] {'kv_1'}, dimensions={0}, use_global_device_ids=true | all-gather | bytes 335360 | tf_op jit(solution)/shard_map/all_gather | solution.py:32
  194.4 0.7 slice_convert_fusion
  195.1 0.2 reshape.1214
  195.2 0.2 fusion.69
  195.4 0.1 copy.175
  195.7 0.1 fusion.64
  195.9 0.1 copy.176
  196.0 0.2 squeeze.185
  196.1 0.1 copy.185
  196.2 0.2 squeeze.187
  196.5 0.2 squeeze.186
  196.7 0.1 copy.186
  196.8 0.2 squeeze.183
  197.0 0.1 copy.167
  197.1 0.2 squeeze.181
  197.4 0.2 squeeze.179
  197.6 0.2 squeeze.178
  197.9 0.1 fusion.77
  198.0 0.1 fusion.75
  198.1 0.1 copy.183
  198.3 0.2 squeeze.188
  198.7 0.1 fusion.67
  198.8 0.2 fusion.52
  199.1 0.1 convolution_convert_fusion.5
  199.3 22.9 %all_to_all.26 = bf16[8,64,128]{2,1,0:T(8,128)(2,1)S(1)} all-to-all(bf16[8,64,128]{2,1,0:T(8,128)(2,1)S(1)} %broadcast_in_dim.71), channel_id=1, replica_groups=mesh['kv_0'=8,'kv_1'=4,'tp'=8] {'tp'}, dimensions={0} | all-to-all | bytes 262144 | tf_op jit(solution)/shard_map/all_to_all | solution.py:52
  222.4 0.6 broadcast_in_dim.73
  223.0 5.5 %all-to-all-start.1 = ((f32[32,1,64]{2,1,0:T(1,128)}), f32[32,1,64]{2,1,0:T(1,128)S(1)}, u32[]{:S(2)}, u32[]{:S(2)}) async-start(f32[32,1,64]{2,1,0:T(1,128)} %broadcast_in_dim.73), calls=%async_computation.1 | async-start | bytes 32768 | tf_op jit(solution)/shard_map/all_to_all | solution.py:52
  228.5 0.2 convolution_convert_fusion
  228.7 0.2 convolution_convert_fusion.1
  229.0 0.9 reshape.1208
  229.8 7.2 %all-to-all-done.1 = f32[32,1,64]{2,1,0:T(1,128)S(1)} async-done(((f32[32,1,64]{2,1,0:T(1,128)}), f32[32,1,64]{2,1,0:T(1,128)S(1)}, u32[]{:S(2)}, u32[]{:S(2)}) %all-to-all-start.1) | async-done | bytes 8224 | tf_op jit(solution)/shard_map/all_to_all | solution.py:52
  237.0 3.9 %all-to-all-start.2 = ((bf16[32,2,2816]{2,1,0:T(2,128)(2,1)}), bf16[32,2,2816]{2,1,0:T(2,128)(2,1)S(1)}, u32[]{:S(2)}, u32[]{:S(2)}) async-start(bf16[32,2,2816]{2,1,0:T(2,128)(2,1)} %reshape.1208), calls=%async_computation.2 | async-start | bytes 720896 | tf_op jit(solution)/shard_map/all_to_all | solution.py:74
  241.0 11.1 %all-to-all-done.2 = bf16[32,2,2816]{2,1,0:T(2,128)(2,1)S(1)} async-done(((bf16[32,2,2816]{2,1,0:T(2,128)(2,1)}), bf16[32,2,2816]{2,1,0:T(2,128)(2,1)S(1)}, u32[]{:S(2)}, u32[]{:S(2)}) %all-to-all-start.2) | async-done | bytes 360480 | tf_op jit(solution)/shard_map/all_to_all | solution.py:74
  252.1 0.3 convert_reduce_fusion
  252.6 15.6 %all_to_all.27 = bf16[32,2,1408]{2,1,0:T(2,128)(2,1)S(1)} all-to-all(bf16[32,2,1408]{2,1,0:T(2,128)(2,1)S(1)} %broadcast_in_dim.74), channel_id=1, replica_groups=mesh['kv_0'=8,'kv_1'=4,'tp'=8] {'kv_0','kv_1'}, dimensions={0} | all-to-all | bytes 360448 | tf_op jit(solution)/shard_map/all_to_all | solution.py:52
  268.3 0.2 convolution_convert_fusion.6
  268.5 11.4 %all_to_all.28 = bf16[8,64,128]{2,1,0:T(8,128)(2,1)S(1)} all-to-all(bf16[8,64,128]{2,1,0:T(8,128)(2,1)S(1)} %broadcast_in_dim.75), channel_id=1, replica_groups=mesh['kv_0'=8,'kv_1'=4,'tp'=8] {'tp'}, dimensions={0} | all-to-all | bytes 262144 | tf_op jit(solution)/shard_map/all_to_all | solution.py:52
  279.9 0.6 fusion.63
  (82 shorter events, 2.4 us)
Async XLA Ops:
  6.5 222.0 %copy-start = (bf16[128,1408]{1,0:T(8,128)(2,1)S(1)}, bf16[128,1408]{1,0:T(8,128)(2,1)}, u32[]{:S(2)}) copy-start(bf16[128,1408]{1,0:T(8,128)(2,1)} %param.30) | copy-start | bytes 1081348
  6.5 148.6 %all-reduce.4.cloned.1.call-start = ((), (), s32[]{:S(2)}) async-start(), calls=%async_computation.5 | async-start | bytes 200704 | tf_op jit(solution)/shard_map/psum | solution.py:17
  12.9 0.6 copy-start.4
  160.5 35.1 %copy-start.6 = (f32[2]{0:T(128)S(1)}, f32[2]{0:T(128)}, u32[]{:S(2)}) copy-start(f32[2]{0:T(128)} %param.22) | copy-start | bytes 28
  161.0 38.1 %copy-start.5 = (bf16[256,128]{1,0:T(8,128)(2,1)S(1)}, bf16[256,128]{1,0:T(8,128)(2,1)}, u32[]{:S(2)}) copy-start(bf16[256,128]{1,0:T(8,128)(2,1)} %param.27) | copy-start | bytes 196612
  161.0 61.2 %copy-start.3 = (bf16[16,4,128]{2,1,0:T(4,128)(2,1)S(1)}, bf16[16,4,128]{2,1,0:T(4,128)(2,1)}, u32[]{:S(2)}) copy-start(bf16[16,4,128]{2,1,0:T(4,128)(2,1)} %param.16) | copy-start | bytes 49156
  161.0 67.4 %copy-start.7 = (f32[128]{0:T(128)S(1)}, f32[128]{0:T(128)}, u32[]{:S(2)}) copy-start(f32[128]{0:T(128)} %param.28) | copy-start | bytes 1540
  164.0 64.7 %copy-start.1 = (bf16[128,1408]{1,0:T(8,128)(2,1)S(1)}, bf16[128,1408]{1,0:T(8,128)(2,1)}, u32[]{:S(2)}) copy-start(bf16[128,1408]{1,0:T(8,128)(2,1)} %param.29) | copy-start | bytes 1081348
  184.4 83.9 %copy-start.2 = (bf16[1408,128]{1,0:T(8,128)(2,1)S(1)}, bf16[1408,128]{1,0:T(8,128)(2,1)}, u32[]{:S(2)}) copy-start(bf16[1408,128]{1,0:T(8,128)(2,1)} %param.31) | copy-start | bytes 1081348
  223.0 14.0 %all-to-all-start.1 = ((f32[32,1,64]{2,1,0:T(1,128)}), f32[32,1,64]{2,1,0:T(1,128)S(1)}, u32[]{:S(2)}, u32[]{:S(2)}) async-start(f32[32,1,64]{2,1,0:T(1,128)} %broadcast_in_dim.73), calls=%async_computation.1 | async-start | bytes 32768 | tf_op jit(solution)/shard_map/all_to_all | solution.py:52
  237.0 15.1 %all-to-all-start.2 = ((bf16[32,2,2816]{2,1,0:T(2,128)(2,1)}), bf16[32,2,2816]{2,1,0:T(2,128)(2,1)S(1)}, u32[]{:S(2)}, u32[]{:S(2)}) async-start(bf16[32,2,2816]{2,1,0:T(2,128)(2,1)} %reshape.1208), calls=%async_computation.2 | async-start | bytes 720896 | tf_op jit(solution)/shard_map/all_to_all | solution.py:74
Sparse Core Ops, SparseCore 0:
  13.7 141.4 all-reduce.3
where the time goes:
time: 288 us; the launch traced here: 287 us
  waiting for transfers between devices  157 us (55%)
  blocking collectives  79.1 us (27%)
  between operations  14 us (5%)
  matrix products  11.2 us (4%)
  starting transfers between devices  9.34 us (3%)
  other arithmetic  8.2 us (3%)
  local copies, waits for them, and re-layouts  8.08 us (3%)
    psum x1, waiting for transfers between devices, in_one(): running = lax.psum(flat, axis)  139 us
    all_to_all x3, blocking collectives, sent_to_all(): lax.all_to_all(jnp.broadcast_to(array[None], (peers, *array.shape)), axis...  49.8 us
    all_gather x2, blocking collectives, all_in_one(): both, at, found = (lax.all_gather(jnp.concatenate(lines), axis), 0, {})  29.3 us
    all_to_all x1, waiting for transfers between devices, sum_at_owner(): lax.all_to_all(tiles, axis, split_axis=0, concat_axis=0, tiled=True)  11.1 us
    all_to_all x1, waiting for transfers between devices, sent_to_all(): lax.all_to_all(jnp.broadcast_to(array[None], (peers, *array.shape)), axis...  7.18 us
  transfers between devices with their start and end apart: 3, of which 3 were waited for; matrix products, arithmetic and copies ran while one was open for 1% of the time, Pallas kernels for 0%

commit v1 on v0

v1 whole, which is shorter than its diff:
```python
import jax
import jax.numpy as jnp
from jax import lax
from jax.experimental import pallas as pl
from jax.experimental.pallas import tpu as pltpu
from jax.sharding import PartitionSpec as P

D = 4096
EPSILON = 1e-06
NEG_FILL = -1e30
SEQS = 16
NEW = 4
ROWS = SEQS * NEW
HEADS = 2
HD = 128
WIDTH = 128
POS = 512
FF = 1408
HALF = 768
SHIFT = FF - HALF
KV = 32
TP = 8
ZS, YS = 8, 4
F32 = jnp.float32
BF16 = jnp.bfloat16
MESH = pl.DeviceIdType.MESH


def far_first(count):
    return sorted(range(1, count), key=lambda d: -min(d, count - d))


OFFSETS = sorted(
    ((dz, dy) for dz in range(ZS) for dy in range(YS) if dz or dy),
    key=lambda o: -(min(o[0], ZS - o[0]) + min(o[1], YS - o[1])),
)


def kernel(
    lengths_ref,
    bias_ref,
    tokens_hbm,
    mix_hbm,
    wq_hbm,
    wk_hbm,
    wv_hbm,
    wf_hbm,
    kc_hbm,
    vc_hbm,
    cg_hbm,
    wo_hbm,
    mlp_hbm,
    wg_hbm,
    wu_hbm,
    wd_hbm,
    out_ref,
    tok,
    mix,
    wq,
    wk,
    wv,
    wf,
    kc,
    vc,
    cg,
    wo,
    mlp,
    wg,
    wu,
    wd,
    xs,
    est,
    qblk,
    att,
    hid,
    send_a,
    recv_a,
    send_q,
    recv_q,
    send_b,
    recv_b,
    send_t,
    recv_t,
    send_c,
    recv_c,
    send_e,
    recv_e,
    send_h,
    recv_h,
    send_f,
    recv_f,
    in_sem,
    send_sem,
    recv_sem,
):
    k = lax.axis_index("kv")
    t = lax.axis_index("tp")
    z, y = k // YS, lax.rem(k, YS)
    head = lax.rem(k, 2)
    mine = k // 2

    loads = {}
    sources = dict(
        tok=(tokens_hbm, tok),
        mix=(mix_hbm, mix),
        wq=(wq_hbm, wq),
        wk=(wk_hbm, wk),
        wv=(wv_hbm, wv),
        wf=(wf_hbm.at[pl.ds(pl.multiple_of(k * WIDTH, WIDTH), WIDTH)], wf),
        kc=(kc_hbm, kc),
        vc=(vc_hbm, vc),
        cg=(cg_hbm, cg),
        wo=(wo_hbm, wo),
        mlp=(mlp_hbm, mlp),
        wg=(wg_hbm, wg),
        wu=(wu_hbm, wu),
        wd=(wd_hbm, wd),
    )
    for n, (name, (src, dst)) in enumerate(sources.items()):
        loads[name] = pltpu.make_async_copy(src, dst, in_sem.at[n])
        loads[name].start()

    kv_peers = [lax.rem(z + dz, ZS) * YS + lax.rem(y + dy, YS) for dz, dy in OFFSETS]
    tp_peers = [lax.rem(t + d, TP) for d in (4, 5, 3, 2, 6, 7, 1)]

    barrier = pltpu.get_barrier_semaphore()
    for peer in kv_peers:
        pl.semaphore_signal(barrier, inc=1, device_id=(peer, t), device_id_type=MESH)
    for peer in tp_peers:
        pl.semaphore_signal(barrier, inc=1, device_id=(k, peer), device_id_type=MESH)

    def to_kv(phase, src, dst, peer):
        pltpu.make_async_remote_copy(
            src_ref=src,
            dst_ref=dst.at[k],
            send_sem=send_sem.at[phase],
            recv_sem=recv_sem.at[phase],
            device_id=(peer, t),
            device_id_type=MESH,
        ).start()

    def to_tp(phase, src, dst):
        for peer in tp_peers:
            pltpu.make_async_remote_copy(
                src_ref=src,
                dst_ref=dst.at[t],
                send_sem=send_sem.at[phase],
                recv_sem=recv_sem.at[phase],
                device_id=(k, peer),
                device_id_type=MESH,
            ).start()

    def arrived(sems, phase, buffer):
        some = buffer.at[pl.ds(0, buffer.shape[0] - 1)]
        pltpu.make_async_copy(some, some, sems.at[phase]).wait()

    for name in ("tok", "mix"):
        loads[name].wait()
    for s in range(SEQS):
        xs[NEW * s : NEW * s + NEW, :] = tok[s].astype(F32)
    x = xs[...]
    scaled = (x * mix[...]).astype(BF16)
    est[...] = jnp.broadcast_to(jnp.sum(x * x, axis=1, keepdims=True), (ROWS, 128))
    loads["wf"].wait()
    est[:, 0:16] = jnp.dot(scaled, wf[...], preferred_element_type=F32)
    for n, (name, w) in enumerate((("wq", wq), ("wk", wk), ("wv", wv))):
        loads[name].wait()
        part = jnp.dot(scaled, w[...], preferred_element_type=F32)
        for s in range(SEQS):
            for h in range(HEADS):
                send_a[2 * s + h, :, HD * n : HD * n + HD] = part[
                    NEW * s : NEW * s + NEW, HD * h : HD * h + HD
                ].astype(BF16)
    for s in range(SEQS):
        piece = est[NEW * s : NEW * s + NEW, :].astype(BF16)
        for h in range(HEADS):
            send_a[2 * s + h, :, 3 * HD : 4 * HD] = piece
    pl.semaphore_wait(barrier, KV - 1 + TP - 1)
    for peer in kv_peers:
        to_kv(0, send_a.at[peer], recv_a, peer)
    recv_a[pl.ds(k, 1)] = send_a[pl.ds(k, 1)]
    qblk[...] = jnp.zeros(qblk.shape, F32)
    arrived(recv_sem, 0, recv_a)
    total = recv_a[0].astype(F32)
    for j in range(1, KV):
        total = total + recv_a[j].astype(F32)
    inv_norm = lax.rsqrt(total[:, 4 * HD - 1 : 4 * HD] / D + EPSILON)
    query = (inv_norm * total[:, 0:HD]).astype(BF16)
    key_new = (inv_norm * total[:, HD : 2 * HD]).astype(BF16).astype(F32)
    value_new = (inv_norm * total[:, 2 * HD : 3 * HD]).astype(BF16).astype(F32)
    lane = lax.broadcasted_iota(jnp.int32, (NEW, 128), 1)
    forget_sum = jnp.sum(
        jnp.where(lane == 2 * t + head, total[:, 3 * HD :], 0.0), axis=1, keepdims=True
    )
    send_q[0] = query
    for peer in kv_peers:
        to_kv(1, send_q.at[0], recv_q, peer)
    recv_q[pl.ds(k, 1)] = query[None]
    gate_in = inv_norm * forget_sum + bias_ref[head]
    log_forget = jnp.minimum(gate_in, 0.0) - jnp.log1p(jnp.exp(-jnp.abs(gate_in)))

    for name in ("kc", "vc", "cg"):
        loads[name].wait()
    arrived(recv_sem, 1, recv_q)
    for s in range(SEQS):
        for h in range(HEADS):
            qblk[s, NEW * h : NEW * h + NEW, HD * h : HD * h + HD] = recv_q[2 * s + h].astype(F32)
    score_scale = HD**-0.5
    position = k * POS + lax.broadcasted_iota(jnp.int32, (8, POS), 1)
    row8 = lax.broadcasted_iota(jnp.int32, (8, POS), 0)
    lane8 = lax.broadcasted_iota(jnp.int32, (8, 128), 1)

    def one_sequence(s):
        length = lengths_ref[s]
        scores = lax.dot_general(
            qblk[s].astype(BF16), kc[s], (((1,), (1,)), ((), ())), preferred_element_type=F32
        )
        both = cg[s]
        cum = jnp.where(row8 < NEW, both[0:1, :], both[1:2, :])
        live = position < length
        scores = jnp.where(live, scores * score_scale - cum, NEG_FILL)
        peak = jnp.max(scores, axis=1, keepdims=True)
        weights = jnp.where(live, jnp.exp(scores - peak), 0.0)
        block_total = jnp.sum(weights, axis=1, keepdims=True)
        block_sum = jnp.dot(weights.astype(BF16), vc[s], preferred_element_type=F32)
        last = jnp.sum(jnp.where(position == length - 1, cum, 0.0), axis=1, keepdims=True)
        stats = jnp.where(
            lane8 == 0, peak, jnp.where(lane8 == 1, block_total, jnp.where(lane8 == 2, last, 0.0))
        )
        for h in range(HEADS):
            lines = slice(NEW * h, NEW * h + NEW)
            send_b[2 * s + h, :, 0:HD] = block_sum[lines, HD * h : HD * h + HD]
            send_b[2 * s + h, :, HD:] = stats[lines]

    def four_sequences(j, carry):
        order = [lax.rem(mine + 8 + 4 * j + u, SEQS) for u in range(4)]
        for s in order:
            one_sequence(s)
        for s in order:
            for h in range(HEADS):
                peer = 2 * s + h

                @pl.when(peer != k)
                def _():
                    to_kv(2, send_b.at[peer], recv_b, peer)

        return carry

    lax.fori_loop(0, 4, four_sequences, 0)
    recv_b[pl.ds(k, 1)] = send_b[pl.ds(k, 1)]
    arrived(recv_sem, 2, recv_b)

    past_peak = recv_b[0, :, HD : HD + 1]
    for j in range(1, KV):
        past_peak = jnp.maximum(past_peak, recv_b[j, :, HD : HD + 1])
    past_total = jnp.zeros((NEW, 1), F32)
    last_cum = jnp.zeros((NEW, 1), F32)
    past_sum = jnp.zeros((NEW, HD), F32)
    for j in range(KV):
        stats = recv_b[j, :, HD:]
        factor = jnp.exp(stats[:, 0:1] - past_peak)
        past_total = past_total + stats[:, 1:2] * factor
        last_cum = last_cum + stats[:, 2:3]
        past_sum = past_sum + recv_b[j, :, 0:HD] * factor
    query_wide = query.astype(F32)
    token = lax.broadcasted_iota(jnp.int32, (NEW, 1), 0)
    key_cum = last_cum[0:1, :]
    own_scores = []
    for i in range(NEW):
        key_cum = key_cum + log_forget[i : i + 1, :]
        dots = jnp.sum(query_wide * key_new[i : i + 1, :], axis=1, keepdims=True)
        own_scores.append(jnp.where(token >= i, dots * score_scale - key_cum, NEG_FILL))
    peak_score = past_peak
    for score in own_scores:
        peak_score = jnp.maximum(peak_score, score)
    past_factor = jnp.exp(past_peak - peak_score)
    numerator = past_sum * past_factor
    denominator = past_total * past_factor
    for i, score in enumerate(own_scores):
        weight = jnp.where(token >= i, jnp.exp(score - peak_score), 0.0)
        numerator = numerator + weight.astype(BF16).astype(F32) * value_new[i : i + 1, :]
        denominator = denominator + weight
    attended = (numerator / denominator).astype(BF16)
    send_t[0] = attended
    for peer in kv_peers:
        to_kv(3, send_t.at[0], recv_t, peer)
    recv_t[pl.ds(k, 1)] = attended[None]
    loads["wo"].wait()
    arrived(recv_sem, 3, recv_t)
    for s in range(SEQS):
        for h in range(HEADS):
            att[NEW * s : NEW * s + NEW, HD * h : HD * h + HD] = recv_t[2 * s + h].astype(F32)

    send_c[0] = jnp.dot(att[...].astype(BF16), wo[...], preferred_element_type=F32).astype(BF16)
    to_tp(4, send_c.at[0], recv_c)
    recv_c[pl.ds(t, 1)] = send_c[...]
    for name in ("mlp", "wg", "wu"):
        loads[name].wait()
    arrived(recv_sem, 4, recv_c)
    attn_out = recv_c[0].astype(F32)
    for j in range(1, TP):
        attn_out = attn_out + recv_c[j].astype(F32)
    middle = (xs[...] + attn_out).astype(BF16).astype(F32)
    xs[...] = middle
    scaled2 = (middle * mlp[...]).astype(BF16)
    squares = jnp.broadcast_to(jnp.sum(middle * middle, axis=1, keepdims=True), (ROWS, 128))
    rough = squares.astype(BF16).astype(F32)
    lane64 = lax.broadcasted_iota(jnp.int32, (ROWS, 128), 1)
    est[...] = jnp.where(lane64 < 64, rough, squares - rough)

    for half in range(2):
        for s in range(SEQS):
            send_e[2 * s + half, :, 2 * HALF :] = est[NEW * s : NEW * s + NEW, :].astype(BF16)
        for n, w in enumerate((wg, wu)):
            for c in range(0, HALF, 256):
                begin = SHIFT * half + c
                part = jnp.dot(scaled2, w[:, begin : begin + 256], preferred_element_type=F32)
                for s in range(SEQS):
                    send_e[2 * s + half, :, HALF * n + c : HALF * n + c + 256] = part[
                        NEW * s : NEW * s + NEW
                    ].astype(BF16)
        for j in range(SEQS):
            peer = 2 * lax.rem(mine + 8 + j, SEQS) + half

            @pl.when(peer != k)
            def _():
                to_kv(5, send_e.at[peer], recv_e, peer)

    recv_e[pl.ds(k, 1)] = send_e[pl.ds(k, 1)]
    arrived(recv_sem, 5, recv_e)
    total = recv_e[0].astype(F32)
    for j in range(1, KV):
        total = total + recv_e[j].astype(F32)
    square_sum = total[:, 2 * HALF : 2 * HALF + 1] + total[:, 2 * HALF + 127 : 2 * HALF + 128]
    inv_norm2 = lax.rsqrt(square_sum / D + EPSILON)
    gate = inv_norm2 * total[:, 0:HALF]
    up = inv_norm2 * total[:, HALF : 2 * HALF]
    hidden = (gate * jax.nn.sigmoid(gate) * up).astype(BF16)
    send_h[0] = hidden
    for peer in kv_peers:
        to_kv(6, send_h.at[0], recv_h, peer)
    recv_h[pl.ds(k, 1)] = hidden[None]
    loads["wd"].wait()
    arrived(recv_sem, 6, recv_h)
    for s in range(SEQS):
        hid[NEW * s : NEW * s + NEW, 0:HALF] = recv_h[2 * s].astype(F32)
        hid[NEW * s : NEW * s + NEW, HALF:] = recv_h[2 * s + 1, :, HALF - SHIFT :].astype(F32)

    send_f[0] = jnp.dot(hid[...].astype(BF16), wd[...], preferred_element_type=F32).astype(BF16)
    to_tp(7, send_f.at[0], recv_f)
    recv_f[pl.ds(t, 1)] = send_f[...]
    arrived(recv_sem, 7, recv_f)
    mixed = recv_f[0].astype(F32)
    for j in range(1, TP):
        mixed = mixed + recv_f[j].astype(F32)
    out_ref[...] = (xs[...] + mixed).astype(BF16)

    for phase, buffer in enumerate(
        (recv_a, recv_q, recv_b, recv_t, recv_c, recv_e, recv_h, recv_f)
    ):
        arrived(send_sem, phase, buffer)


def on_device(
    tokens,
    mix_gain,
    w_query,
    w_key,
    w_value,
    w_forget,
    forget_bias,
    key_cache,
    value_cache,
    cum_gate,
    lengths,
    w_out,
    mlp_gain,
    w_gate,
    w_up,
    w_down,
):
    in_vmem = [
        tokens,
        mix_gain.reshape(1, WIDTH),
        w_query,
        w_key,
        w_value,
        w_forget,
        key_cache,
        value_cache,
        cum_gate,
        w_out,
        mlp_gain.reshape(1, WIDTH),
        w_gate,
        w_up,
        w_down,
    ]
    shapes = [pltpu.VMEM(a.shape, a.dtype) for a in in_vmem]
    shapes[5] = pltpu.VMEM((WIDTH, 16), BF16)
    out = pl.pallas_call(
        kernel,
        out_shape=jax.ShapeDtypeStruct((ROWS, WIDTH), BF16),
        in_specs=[pl.BlockSpec(memory_space=pltpu.SMEM)] * 2
        + [pl.BlockSpec(memory_space=pl.ANY)] * len(in_vmem),
        out_specs=pl.BlockSpec(memory_space=pltpu.VMEM),
        scratch_shapes=shapes
        + [
            pltpu.VMEM((ROWS, WIDTH), F32),
            pltpu.VMEM((ROWS, 128), F32),
            pltpu.VMEM((SEQS, 8, 2 * HD), F32),
            pltpu.VMEM((ROWS, 2 * HD), F32),
            pltpu.VMEM((ROWS, FF), F32),
            pltpu.VMEM((KV, NEW, 4 * HD), BF16),
            pltpu.VMEM((KV, NEW, 4 * HD), BF16),
            pltpu.VMEM((1, NEW, HD), BF16),
            pltpu.VMEM((KV, NEW, HD), BF16),
            pltpu.VMEM((KV, NEW, 2 * HD), F32),
            pltpu.VMEM((KV, NEW, 2 * HD), F32),
            pltpu.VMEM((1, NEW, HD), BF16),
            pltpu.VMEM((KV, NEW, HD), BF16),
            pltpu.VMEM((1, ROWS, WIDTH), BF16),
            pltpu.VMEM((TP, ROWS, WIDTH), BF16),
            pltpu.VMEM((KV, NEW, 2 * HALF + 128), BF16),
            pltpu.VMEM((KV, NEW, 2 * HALF + 128), BF16),
            pltpu.VMEM((1, NEW, HALF), BF16),
            pltpu.VMEM((KV, NEW, HALF), BF16),
            pltpu.VMEM((1, ROWS, WIDTH), BF16),
            pltpu.VMEM((TP, ROWS, WIDTH), BF16),
            pltpu.SemaphoreType.DMA((len(in_vmem),)),
            pltpu.SemaphoreType.DMA((8,)),
            pltpu.SemaphoreType.DMA((8,)),
        ],
        compiler_params=pltpu.CompilerParams(
            collective_id=0, has_side_effects=True, vmem_limit_bytes=48 * 1024 * 1024
        ),
    )(lengths, forget_bias, *in_vmem)
    return out.reshape(SEQS, NEW, WIDTH)


def solution(mesh):
    return jax.shard_map(
        on_device,
        mesh=mesh,
        in_specs=(
            P(None, None, "kv"),
            P("kv"),
            P("kv", "tp"),
            P("kv", "tp"),
            P("kv", "tp"),
            P(),
            P("tp"),
            P(None, "kv", "tp"),
            P(None, "kv", "tp"),
            P(None, "tp", "kv"),
            P(),
            P("tp", "kv"),
            P("kv"),
            P("kv", "tp"),
            P("kv", "tp"),
            P("tp", "kv"),
        ),
        out_specs=P(None, None, "kv"),
        check_vma=False,
    )
```

time: 288 us -> 84.7 us (0.29)
  waiting for transfers between devices: 157 us -> 0 us
  blocking collectives: 79.1 us -> 0 us
  Pallas kernels: 0 us -> 71.6 us
  between operations: 14 us -> 0.04 us
  matrix products: 11.2 us -> 0 us
  starting transfers between devices: 9.34 us -> 0 us
  other arithmetic: 8.2 us -> 0 us
  local copies, waits for them, and re-layouts: 8.08 us -> 12.5 us
    psum x1 -> x0, waiting for transfers between devices: 139 us -> none  [in_one(): running = lax.psum(flat, axis)]
    pallas_call x0 -> x1, Pallas kernels: none -> 71.6 us  [on_device(): pl.pallas_call(kernel, out_shape=jax.ShapeDtypeStruct((ROWS, WIDTH), BF16...]
    all_to_all x3 -> x0, blocking collectives: 49.8 us -> none  [sent_to_all(): lax.all_to_all(jnp.broadcast_to(array[None], (peers, *array.shape)), axis...]
    all_gather x2 -> x0, blocking collectives: 29.3 us -> none  [all_in_one(): both, at, found = (lax.all_gather(jnp.concatenate(lines), axis), 0, {})]
    all_to_all x2 -> x0, waiting for transfers between devices: 18.3 us -> none  [the longest x1 11.1 us: sum_at_owner(): lax.all_to_all(tiles, axis, split_axis=0, concat_axis=0, tiled=True)]
    unnamed x23 -> x28, local copies, waits for them, and re-layouts: 1.05 us -> 12.5 us
    dot_general x12 -> x0, matrix products: 11.2 us -> none  [the longest x1 3.47 us: on_device(): jnp.einsum('bthd,bphd->bthp', query, cached_keys, preferred_element_type=...]
    all_to_all x2 -> x0, starting transfers between devices: 9.34 us -> none  [the longest x1 5.47 us: sent_to_all(): lax.all_to_all(jnp.broadcast_to(array[None], (peers, *array.shape)), axis...]
  transfers between devices with their start and end apart: 3 -> 0, of which waited for: 3 -> 0; matrix products, arithmetic and copies ran while one was open for 1% -> 0% of each run, Pallas kernels for 0% -> 0%
where the time goes in v1:
time: 84.7 us; the launch traced here: 84.1 us
  Pallas kernels  71.6 us (85%)
  local copies, waits for them, and re-layouts  12.5 us (15%)
    pallas_call x1, Pallas kernels, on_device(): pl.pallas_call(kernel, out_shape=jax.ShapeDtypeStruct((ROWS, WIDTH), BF16...  71.6 us
    unnamed x28, local copies, waits for them, and re-layouts  12.5 us

profile of v1, /device:TPU:1, one launch (start us, length us, event | category | flops | bytes accessed | tf_op | source)
XLA Modules:
  0.0 84.1 jit_solution(14271735080741148644)
XLA Ops:
  0.0 1.4 %copy.17.wf_hbm = bf16[4096,16]{1,0:T(8,128)(2,1)S(1)} copy(bf16[4096,16]{0,1:T(8,128)(2,1)} %param.21) | data formatting | bytes 262144 | tf_op args[5]
  1.4 0.0 copy-start
  1.4 1.0 %copy-done = bf16[128,1408]{1,0:T(8,128)(2,1)S(1)} copy-done((bf16[128,1408]{1,0:T(8,128)(2,1)S(1)}, bf16[128,1408]{1,0:T(8,128)(2,1)}, u32[]{:S(2)}) %copy-start) | copy-done | bytes 360472
  2.4 0.0 copy-start.1
  2.4 1.0 %copy-done.1 = bf16[128,1408]{1,0:T(8,128)(2,1)S(1)} copy-done((bf16[128,1408]{1,0:T(8,128)(2,1)S(1)}, bf16[128,1408]{1,0:T(8,128)(2,1)}, u32[]{:S(2)}) %copy-start.1) | copy-done | bytes 360472
  3.4 0.0 copy-start.2
  3.4 1.0 %copy-done.2 = bf16[1408,128]{1,0:T(8,128)(2,1)S(1)} copy-done((bf16[1408,128]{1,0:T(8,128)(2,1)S(1)}, bf16[1408,128]{1,0:T(8,128)(2,1)}, u32[]{:S(2)}) %copy-start.2) | copy-done | bytes 360472
  4.3 0.0 copy-start.3
  4.3 0.8 copy-done.3
  5.2 0.0 copy-start.4
  5.2 0.8 copy-done.4
  6.0 0.0 copy-start.5
  6.0 0.8 copy-done.5
  6.9 0.0 copy-start.6
  6.9 0.8 copy-done.6
  7.7 0.0 copy-start.7
  7.7 0.8 copy-done.7
  8.5 0.0 copy-start.8
  8.5 0.7 copy-done.8
  9.3 0.0 copy-start.9
  9.3 0.7 copy-done.9
  9.9 0.0 copy-start.10
  9.9 0.7 copy-done.10
  10.6 0.0 copy-start.11
  10.6 0.7 copy-done.11
  11.2 0.0 copy-start.12
  11.2 0.7 copy-done.12
  11.9 71.6 %shard_map.154 = bf16[64,128]{1,0:T(8,128)(2,1)S(1)} custom-call(s32[16]{0:T(128)S(1)} %copy-done.9, f32[2]{0:T(128)S(1)} %copy-done.10, bf16[16,4,128]{2,1,0:T(4,128)(2,1)S(1)} %copy-done.8, f32[1,128]{1,0:T(1,128)S(1)} %bitcast.4, bf16[128,256]{1,0:T(8,128)(2,1)S(1)} %copy-done.3, bf16[128,256]{1,0:T(8,128)(2,1)S(1)} %copy-done.4, ...), custom_call_target="tpu_custom_call" | custom-call | tf_op jit(solution)/shard_map/pallas_call | solution.py:400
  83.5 0.6 copy.19
Async XLA Ops:
  1.4 1.0 %copy-start = (bf16[128,1408]{1,0:T(8,128)(2,1)S(1)}, bf16[128,1408]{1,0:T(8,128)(2,1)}, u32[]{:S(2)}) copy-start(bf16[128,1408]{1,0:T(8,128)(2,1)} %wg_hbm.1) | copy-start | bytes 1081348
  2.4 1.0 %copy-start.1 = (bf16[128,1408]{1,0:T(8,128)(2,1)S(1)}, bf16[128,1408]{1,0:T(8,128)(2,1)}, u32[]{:S(2)}) copy-start(bf16[128,1408]{1,0:T(8,128)(2,1)} %wu_hbm.1) | copy-start | bytes 1081348
  3.4 1.0 %copy-start.2 = (bf16[1408,128]{1,0:T(8,128)(2,1)S(1)}, bf16[1408,128]{1,0:T(8,128)(2,1)}, u32[]{:S(2)}) copy-start(bf16[1408,128]{1,0:T(8,128)(2,1)} %wd_hbm.1) | copy-start | bytes 1081348
  4.3 0.8 copy-start.3
  5.2 0.8 copy-start.4
  6.0 0.8 copy-start.5
  6.9 0.8 copy-start.6
  7.7 0.8 copy-start.7
  8.5 0.7 copy-start.8
  9.3 0.7 copy-start.9
  9.9 0.7 copy-start.10
  10.6 0.7 copy-start.11
  11.2 0.7 copy-start.12

commit v2 on v1

--- a/solution.py
+++ b/solution.py
@@ -8,6 +8,7 @@
 D = 4096
 EPSILON = 1e-06
 NEG_FILL = -1e30
+PEAK_FLOOR = -1e29
 SEQS = 16
 NEW = 4
 ROWS = SEQS * NEW
@@ -16,18 +17,16 @@
 WIDTH = 128
 POS = 512
 FF = 1408
-HALF = 768
-SHIFT = FF - HALF
+CUT = 768
+FIRST = 384
+EARLY = 128 + 2 * FIRST
+LATE = (2 * (CUT - FIRST), 2 * (FF - CUT - FIRST))
 KV = 32
 TP = 8
 ZS, YS = 8, 4
 F32 = jnp.float32
 BF16 = jnp.bfloat16
 MESH = pl.DeviceIdType.MESH
-
-
-def far_first(count):
-    return sorted(range(1, count), key=lambda d: -min(d, count - d))
 
 
 OFFSETS = sorted(
@@ -71,6 +70,8 @@
     xs,
     est,
     qblk,
+    bias,
+    last,
     att,
     hid,
     send_a,
@@ -85,8 +86,12 @@
     recv_c,
     send_e,
     recv_e,
+    send_l,
+    recv_l,
     send_h,
     recv_h,
+    send_m,
+    recv_m,
     send_f,
     recv_f,
     in_sem,
@@ -106,7 +111,7 @@
         wq=(wq_hbm, wq),
         wk=(wk_hbm, wk),
         wv=(wv_hbm, wv),
-        wf=(wf_hbm.at[pl.ds(pl.multiple_of(k * WIDTH, WIDTH), WIDTH)], wf),
+        wf=(wf_hbm.at[:, pl.ds(pl.multiple_of(k * WIDTH, WIDTH), WIDTH)], wf),
         kc=(kc_hbm, kc),
         vc=(vc_hbm, vc),
         cg=(cg_hbm, cg),
@@ -139,6 +144,16 @@
             device_id_type=MESH,
         ).start()
 
+    def to_kv_part(phase, src, dst, peer, width, at=None):
+        pltpu.make_async_remote_copy(
+            src_ref=src.at[peer if at is None else at, :, pl.ds(0, width)],
+            dst_ref=dst.at[k, :, pl.ds(0, width)],
+            send_sem=send_sem.at[phase],
+            recv_sem=recv_sem.at[phase],
+            device_id=(peer, t),
+            device_id_type=MESH,
+        ).start()
+
     def to_tp(phase, src, dst):
         for peer in tp_peers:
             pltpu.make_async_remote_copy(
@@ -152,7 +167,8 @@
 
     def arrived(sems, phase, buffer):
         some = buffer.at[pl.ds(0, buffer.shape[0] - 1)]
-        pltpu.make_async_copy(some, some, sems.at[phase]).wait()
+        with jax.named_scope(("recv%d" if sems is recv_sem else "sent%d") % phase):
+            pltpu.make_async_copy(some, some, sems.at[phase]).wait()
 
     for name in ("tok", "mix"):
         loads[name].wait()
@@ -162,7 +178,9 @@
     scaled = (x * mix[...]).astype(BF16)
     est[...] = jnp.broadcast_to(jnp.sum(x * x, axis=1, keepdims=True), (ROWS, 128))
     loads["wf"].wait()
-    est[:, 0:16] = jnp.dot(scaled, wf[...], preferred_element_type=F32)
+    est[:, 0:16] = lax.dot_general(
+        scaled, wf[...], (((1,), (1,)), ((), ())), preferred_element_type=F32
+    )
     for n, (name, w) in enumerate((("wq", wq), ("wk", wk), ("wv", wv))):
         loads[name].wait()
         part = jnp.dot(scaled, w[...], preferred_element_type=F32)
@@ -175,11 +193,25 @@
         piece = est[NEW * s : NEW * s + NEW, :].astype(BF16)
         for h in range(HEADS):
             send_a[2 * s + h, :, 3 * HD : 4 * HD] = piece
-    pl.semaphore_wait(barrier, KV - 1 + TP - 1)
+    with jax.named_scope("barrier"):
+        pl.semaphore_wait(barrier, KV - 1 + TP - 1)
     for peer in kv_peers:
         to_kv(0, send_a.at[peer], recv_a, peer)
     recv_a[pl.ds(k, 1)] = send_a[pl.ds(k, 1)]
     qblk[...] = jnp.zeros(qblk.shape, F32)
+    for name in ("kc", "vc", "cg"):
+        loads[name].wait()
+    score_scale = HD**-0.5
+    position = k * POS + lax.broadcasted_iota(jnp.int32, (8, POS), 1)
+    row8 = lax.broadcasted_iota(jnp.int32, (8, POS), 0)
+    lane8 = lax.broadcasted_iota(jnp.int32, (8, 128), 1)
+    for s in range(SEQS):
+        length = lengths_ref[s]
+        both = cg[s]
+        cum = jnp.where(row8 < NEW, both[0:1, :], both[1:2, :])
+        bias[s] = jnp.where(position < length, -cum, NEG_FILL)
+        at_last = jnp.sum(jnp.where(position == length - 1, cum, 0.0), axis=1, keepdims=True)
+        last[s] = jnp.broadcast_to(at_last, (8, 128))
     arrived(recv_sem, 0, recv_a)
     total = recv_a[0].astype(F32)
     for j in range(1, KV):
@@ -199,54 +231,30 @@
     gate_in = inv_norm * forget_sum + bias_ref[head]
     log_forget = jnp.minimum(gate_in, 0.0) - jnp.log1p(jnp.exp(-jnp.abs(gate_in)))
 
-    for name in ("kc", "vc", "cg"):
-        loads[name].wait()
     arrived(recv_sem, 1, recv_q)
     for s in range(SEQS):
         for h in range(HEADS):
             qblk[s, NEW * h : NEW * h + NEW, HD * h : HD * h + HD] = recv_q[2 * s + h].astype(F32)
-    score_scale = HD**-0.5
-    position = k * POS + lax.broadcasted_iota(jnp.int32, (8, POS), 1)
-    row8 = lax.broadcasted_iota(jnp.int32, (8, POS), 0)
-    lane8 = lax.broadcasted_iota(jnp.int32, (8, 128), 1)
-
-    def one_sequence(s):
-        length = lengths_ref[s]
-        scores = lax.dot_general(
-            qblk[s].astype(BF16), kc[s], (((1,), (1,)), ((), ())), preferred_element_type=F32
-        )
-        both = cg[s]
-        cum = jnp.where(row8 < NEW, both[0:1, :], both[1:2, :])
-        live = position < length
-        scores = jnp.where(live, scores * score_scale - cum, NEG_FILL)
-        peak = jnp.max(scores, axis=1, keepdims=True)
-        weights = jnp.where(live, jnp.exp(scores - peak), 0.0)
-        block_total = jnp.sum(weights, axis=1, keepdims=True)
-        block_sum = jnp.dot(weights.astype(BF16), vc[s], preferred_element_type=F32)
-        last = jnp.sum(jnp.where(position == length - 1, cum, 0.0), axis=1, keepdims=True)
-        stats = jnp.where(
-            lane8 == 0, peak, jnp.where(lane8 == 1, block_total, jnp.where(lane8 == 2, last, 0.0))
-        )
-        for h in range(HEADS):
-            lines = slice(NEW * h, NEW * h + NEW)
-            send_b[2 * s + h, :, 0:HD] = block_sum[lines, HD * h : HD * h + HD]
-            send_b[2 * s + h, :, HD:] = stats[lines]
-
-    def four_sequences(j, carry):
-        order = [lax.rem(mine + 8 + 4 * j + u, SEQS) for u in range(4)]
-        for s in order:
-            one_sequence(s)
-        for s in order:
+    for dz in (4, 5, 3, 6, 2, 7, 1, 0):
+        z_peer = lax.rem(z + dz, ZS)
+        for s in (2 * z_peer, 2 * z_peer + 1):
+            scores = lax.dot_general(
+                qblk[s].astype(BF16), kc[s], (((1,), (1,)), ((), ())), preferred_element_type=F32
+            )
+            scores = scores * score_scale + bias[s]
+            peak = jnp.maximum(jnp.max(scores, axis=1, keepdims=True), PEAK_FLOOR)
+            weights = jnp.exp(scores - peak)
+            block_total = jnp.sum(weights, axis=1, keepdims=True)
+            block_sum = jnp.dot(weights.astype(BF16), vc[s], preferred_element_type=F32)
+            stats = jnp.where(lane8 == 0, peak, jnp.where(lane8 == 1, block_total, last[s]))
             for h in range(HEADS):
-                peer = 2 * s + h
-
-                @pl.when(peer != k)
-                def _():
-                    to_kv(2, send_b.at[peer], recv_b, peer)
-
-        return carry
-
-    lax.fori_loop(0, 4, four_sequences, 0)
+                lines = slice(NEW * h, NEW * h + NEW)
+                send_b[2 * s + h, :, 0:HD] = block_sum[lines, HD * h : HD * h + HD]
+                send_b[2 * s + h, :, HD:] = stats[lines]
+        for dy in (2, 1, 3, 0):
+            if dz or dy:
+                peer = z_peer * YS + lax.rem(y + dy, YS)
+                to_kv(2, send_b.at[peer], recv_b, peer)
     recv_b[pl.ds(k, 1)] = send_b[pl.ds(k, 1)]
     arrived(recv_sem, 2, recv_b)
 
@@ -308,43 +316,87 @@
     lane64 = lax.broadcasted_iota(jnp.int32, (ROWS, 128), 1)
     est[...] = jnp.where(lane64 < 64, rough, squares - rough)
 
+    for s in range(SEQS):
+        piece = est[NEW * s : NEW * s + NEW, :].astype(BF16)
+        for half in range(2):
+            send_e[2 * s + half, :, 0:128] = piece
+
+    def partial_products(dst, at, begin, width, half):
+        for n, w in enumerate((wg, wu)):
+            part = jnp.dot(scaled2, w[:, begin : begin + width], preferred_element_type=F32)
+            for s in range(SEQS):
+                dst[2 * s + half, :, at + width * n : at + width * n + width] = part[
+                    NEW * s : NEW * s + NEW
+                ].astype(BF16)
+
     for half in range(2):
-        for s in range(SEQS):
-            send_e[2 * s + half, :, 2 * HALF :] = est[NEW * s : NEW * s + NEW, :].astype(BF16)
-        for n, w in enumerate((wg, wu)):
-            for c in range(0, HALF, 256):
-                begin = SHIFT * half + c
-                part = jnp.dot(scaled2, w[:, begin : begin + 256], preferred_element_type=F32)
-                for s in range(SEQS):
-                    send_e[2 * s + half, :, HALF * n + c : HALF * n + c + 256] = part[
-                        NEW * s : NEW * s + NEW
-                    ].astype(BF16)
-        for j in range(SEQS):
-            peer = 2 * lax.rem(mine + 8 + j, SEQS) + half
-
-            @pl.when(peer != k)
+        partial_products(send_e, 128, CUT * half, FIRST, half)
+    for peer in kv_peers:
+        to_kv(5, send_e.at[peer], recv_e, peer)
+    for half in range(2):
+        partial_products(send_l, 0, CUT * half + FIRST, LATE[half] // 2, half)
+    for dz, dy in OFFSETS:
+        peer = lax.rem(z + dz, ZS) * YS + lax.rem(y + dy, YS)
+        half = lax.rem(y + dy, 2)
+        for h in range(2):
+
+            @pl.when(half == h)
             def _():
-                to_kv(5, send_e.at[peer], recv_e, peer)
+                to_kv_part(8, send_l, recv_l, peer, LATE[h])
 
     recv_e[pl.ds(k, 1)] = send_e[pl.ds(k, 1)]
+    recv_l[pl.ds(k, 1)] = send_l[pl.ds(k, 1)]
     arrived(recv_sem, 5, recv_e)
     total = recv_e[0].astype(F32)
     for j in range(1, KV):
         total = total + recv_e[j].astype(F32)
-    square_sum = total[:, 2 * HALF : 2 * HALF + 1] + total[:, 2 * HALF + 127 : 2 * HALF + 128]
-    inv_norm2 = lax.rsqrt(square_sum / D + EPSILON)
-    gate = inv_norm2 * total[:, 0:HALF]
-    up = inv_norm2 * total[:, HALF : 2 * HALF]
-    hidden = (gate * jax.nn.sigmoid(gate) * up).astype(BF16)
+    inv_norm2 = lax.rsqrt((total[:, 0:1] + total[:, 127:128]) / D + EPSILON)
+
+    def hidden_of(gate, up):
+        gate = inv_norm2 * gate
+        return (gate * jax.nn.sigmoid(gate) * (inv_norm2 * up)).astype(BF16)
+
+    hidden = hidden_of(total[:, 128 : 128 + FIRST], total[:, 128 + FIRST :])
     send_h[0] = hidden
     for peer in kv_peers:
         to_kv(6, send_h.at[0], recv_h, peer)
     recv_h[pl.ds(k, 1)] = hidden[None]
+    for h in range(2):
+
+        @pl.when(head == h)
+        def _():
+            width = LATE[h]
+            with jax.named_scope("recv8"):
+                some = recv_l.at[pl.ds(0, KV - 1), :, pl.ds(0, width)]
+                pltpu.make_async_copy(some, some, recv_sem.at[8]).wait()
+            total = recv_l[0, :, 0:width].astype(F32)
+            for j in range(1, KV):
+                total = total + recv_l[j, :, 0:width].astype(F32)
+            hidden = hidden_of(total[:, 0 : width // 2], total[:, width // 2 :])
+            send_m[0, :, 0 : width // 2] = hidden
+            recv_m[pl.ds(k, 1), :, 0 : width // 2] = hidden[None]
+            for peer in kv_peers:
+                to_kv_part(9, send_m, recv_m, peer, width // 2, 0)
+
     loads["wd"].wait()
     arrived(recv_sem, 6, recv_h)
     for s in range(SEQS):
-        hid[NEW * s : NEW * s + NEW, 0:HALF] = recv_h[2 * s].astype(F32)
-        hid[NEW * s : NEW * s + NEW, HALF:] = recv_h[2 * s + 1, :, HALF - SHIFT :].astype(F32)
+        for h in range(2):
+            hid[NEW * s : NEW * s + NEW, CUT * h : CUT * h + FIRST] = recv_h[2 * s + h].astype(F32)
+    enough = (recv_e.at[pl.ds(0, 11)], recv_l.at[pl.ds(0, 13)])
+    for h in range(2):
+
+        @pl.when(head == h)
+        def _():
+            with jax.named_scope("recv9"):
+                pltpu.make_async_copy(enough[h], enough[h], recv_sem.at[9]).wait()
+
+    for s in range(SEQS):
+        for h in range(2):
+            begin, width = CUT * h + FIRST, LATE[h] // 2
+            hid[NEW * s : NEW * s + NEW, begin : begin + width] = recv_m[
+                2 * s + h, :, 0:width
+            ].astype(F32)
 
     send_f[0] = jnp.dot(hid[...].astype(BF16), wd[...], preferred_element_type=F32).astype(BF16)
     to_tp(7, send_f.at[0], recv_f)
@@ -359,6 +411,14 @@
         (recv_a, recv_q, recv_b, recv_t, recv_c, recv_e, recv_h, recv_f)
     ):
         arrived(send_sem, phase, buffer)
+    enough = (recv_e.at[pl.ds(0, 22)], recv_l.at[pl.ds(0, 26)])
+    for h in range(2):
+
+        @pl.when(head == h)
+        def _():
+            pltpu.make_async_copy(enough[h], enough[h], send_sem.at[8]).wait()
+            some = recv_m.at[pl.ds(0, KV - 1), :, pl.ds(0, LATE[h] // 2)]
+            pltpu.make_async_copy(some, some, send_sem.at[9]).wait()
 
 
 def on_device(
@@ -385,7 +445,7 @@
         w_query,
         w_key,
         w_value,
-        w_forget,
+        w_forget.T,
         key_cache,
         value_cache,
         cum_gate,
@@ -396,18 +456,20 @@
         w_down,
     ]
     shapes = [pltpu.VMEM(a.shape, a.dtype) for a in in_vmem]
-    shapes[5] = pltpu.VMEM((WIDTH, 16), BF16)
+    shapes[5] = pltpu.VMEM((16, WIDTH), BF16)
     out = pl.pallas_call(
         kernel,
         out_shape=jax.ShapeDtypeStruct((ROWS, WIDTH), BF16),
         in_specs=[pl.BlockSpec(memory_space=pltpu.SMEM)] * 2
-        + [pl.BlockSpec(memory_space=pl.ANY)] * len(in_vmem),
+        + [pl.BlockSpec(memory_space=pltpu.HBM)] * len(in_vmem),
         out_specs=pl.BlockSpec(memory_space=pltpu.VMEM),
         scratch_shapes=shapes
         + [
             pltpu.VMEM((ROWS, WIDTH), F32),
             pltpu.VMEM((ROWS, 128), F32),
             pltpu.VMEM((SEQS, 8, 2 * HD), F32),
+            pltpu.VMEM((SEQS, 8, POS), F32),
+            pltpu.VMEM((SEQS, 8, 128), F32),
             pltpu.VMEM((ROWS, 2 * HD), F32),
             pltpu.VMEM((ROWS, FF), F32),
             pltpu.VMEM((KV, NEW, 4 * HD), BF16),
@@ -420,18 +482,22 @@
             pltpu.VMEM((KV, NEW, HD), BF16),
             pltpu.VMEM((1, ROWS, WIDTH), BF16),
             pltpu.VMEM((TP, ROWS, WIDTH), BF16),
-            pltpu.VMEM((KV, NEW, 2 * HALF + 128), BF16),
-            pltpu.VMEM((KV, NEW, 2 * HALF + 128), BF16),
-            pltpu.VMEM((1, NEW, HALF), BF16),
-            pltpu.VMEM((KV, NEW, HALF), BF16),
+            pltpu.VMEM((KV, NEW, EARLY), BF16),
+            pltpu.VMEM((KV, NEW, EARLY), BF16),
+            pltpu.VMEM((KV, NEW, LATE[0]), BF16),
+            pltpu.VMEM((KV, NEW, LATE[0]), BF16),
+            pltpu.VMEM((1, NEW, FIRST), BF16),
+            pltpu.VMEM((KV, NEW, FIRST), BF16),
+            pltpu.VMEM((1, NEW, LATE[0] // 2), BF16),
+            pltpu.VMEM((KV, NEW, LATE[0] // 2), BF16),
             pltpu.VMEM((1, ROWS, WIDTH), BF16),
             pltpu.VMEM((TP, ROWS, WIDTH), BF16),
             pltpu.SemaphoreType.DMA((len(in_vmem),)),
-            pltpu.SemaphoreType.DMA((8,)),
-            pltpu.SemaphoreType.DMA((8,)),
+            pltpu.SemaphoreType.DMA((10,)),
+            pltpu.SemaphoreType.DMA((10,)),
         ],
         compiler_params=pltpu.CompilerParams(
-            collective_id=0, has_side_effects=True, vmem_limit_bytes=48 * 1024 * 1024
+            collective_id=0, has_side_effects=True, vmem_limit_bytes=67043328
         ),
     )(lengths, forget_bias, *in_vmem)
     return out.reshape(SEQS, NEW, WIDTH)

time: 84.7 us -> 67.8 us (0.80)
  local copies, waits for them, and re-layouts: 12.5 us -> 1.33 us
  Pallas kernels: 71.6 us -> 66.2 us
    unnamed x28 -> x1, local copies, waits for them, and re-layouts: 12.5 us -> 1.33 us
    pallas_call x1, Pallas kernels: 71.6 us -> 66.2 us  [on_device(): pl.pallas_call(kernel, out_shape=jax.ShapeDtypeStruct((ROWS, WIDTH), BF16...]
where the time goes in v2:
time: 67.8 us; the launch traced here: 67.5 us
  Pallas kernels  66.2 us (98%)
  local copies, waits for them, and re-layouts  1.33 us (2%)
    pallas_call x1, Pallas kernels, on_device(): pl.pallas_call(kernel, out_shape=jax.ShapeDtypeStruct((ROWS, WIDTH), BF16...  66.2 us

profile of v2, /device:TPU:1, one launch (start us, length us, event | category | flops | bytes accessed | tf_op | source)
XLA Modules:
  0.0 67.5 jit_solution(3434214304205195904)
XLA Ops:
  0.0 66.2 %shard_map.154 = bf16[64,128]{1,0:T(8,128)(2,1)} custom-call(s32[16]{0:T(128)} %lengths_ref.1, f32[2]{0:T(128)} %bias_ref.1, bf16[16,4,128]{2,1,0:T(4,128)(2,1)} %tokens_hbm.1, f32[1,128]{1,0:T(1,128)} %bitcast.6, bf16[128,256]{1,0:T(8,128)(2,1)} %wq_hbm.1, bf16[128,256]{1,0:T(8,128)(2,1)} %wk_hbm.1, bf16[128,256]{1,0:T(8,128)(2,1)} %wv_hbm.1, ...), custom_call_target="tpu_custom_call" | custom-call | tf_op jit(solution)/shard_map/pallas_call | solution.py:460
  66.2 1.3 %copy.18 = bf16[16,4,128]{2,1,0:T(4,128)(2,1)} copy(bf16[16,4,128]{2,1,0:T(4,128)(2,1)} %bitcast.5) | data formatting | bytes 32768

commit v3 on v2

v3 whole, which is shorter than its diff:
```python
import jax
import jax.numpy as jnp
from jax import lax
from jax.experimental import pallas as pl
from jax.experimental.pallas import tpu as pltpu
from jax.sharding import PartitionSpec as P

D = 4096
EPSILON = 1e-06
NEG_FILL = -1e30
PEAK_FLOOR = -1e29
SEQS = 16
NEW = 4
ROWS = SEQS * NEW
HEADS = 2
HD = 128
WIDTH = 128
POS = 512
FF = 1408
CUT = 768
FIRST = 384
EARLY = 128 + 2 * FIRST
LATE = (2 * (CUT - FIRST), 2 * (FF - CUT - FIRST))
KV = 32
TP = 8
ZS, YS = 8, 4
F32 = jnp.float32
BF16 = jnp.bfloat16
MESH = pl.DeviceIdType.MESH


OFFSETS = sorted(
    ((dz, dy) for dz in range(ZS) for dy in range(YS) if dz or dy),
    key=lambda o: -(min(o[0], ZS - o[0]) + min(o[1], YS - o[1])),
)


def kernel(
    lengths_ref,
    bias_ref,
    tokens_hbm,
    mix_hbm,
    wq_hbm,
    wk_hbm,
    wv_hbm,
    wf_hbm,
    kc_hbm,
    vc_hbm,
    cg_hbm,
    wo_hbm,
    mlp_hbm,
    wg_hbm,
    wu_hbm,
    wd_hbm,
    out_ref,
    tok,
    mix,
    wq,
    wk,
    wv,
    wf,
    kc,
    vc,
    cg,
    wo,
    mlp,
    wg,
    wu,
    wd,
    xs,
    est,
    qblk,
    kt,
    bias,
    last,
    att,
    hid,
    state,
    send_a,
    recv_a,
    send_q,
    recv_q,
    send_b,
    recv_b,
    send_t,
    recv_t,
    send_c,
    recv_c,
    send_e,
    recv_e,
    send_l,
    recv_l,
    send_h,
    recv_h,
    send_m,
    recv_m,
    send_f,
    recv_f,
    in_sem,
    send_sem,
    recv_sem,
):
    k = lax.axis_index("kv")
    t = lax.axis_index("tp")
    z, y = k // YS, lax.rem(k, YS)
    head = lax.rem(k, 2)
    mine = k // 2

    loads = {}
    sources = dict(
        tok=(tokens_hbm, tok),
        mix=(mix_hbm, mix),
        wq=(wq_hbm, wq),
        wk=(wk_hbm, wk),
        wv=(wv_hbm, wv),
        wf=(wf_hbm.at[:, pl.ds(pl.multiple_of(k * WIDTH, WIDTH), WIDTH)], wf),
        kc=(kc_hbm, kc),
        vc=(vc_hbm, vc),
        cg=(cg_hbm, cg),
        wo=(wo_hbm, wo),
        mlp=(mlp_hbm, mlp),
        wg=(wg_hbm, wg),
        wu=(wu_hbm, wu),
        wd=(wd_hbm, wd),
    )
    kv_peers = [lax.rem(z + dz, ZS) * YS + lax.rem(y + dy, YS) for dz, dy in OFFSETS]
    tp_peers = [lax.rem(t + d, TP) for d in (4, 5, 3, 2, 6, 7, 1)]
    core = lax.rem(t, 2)
    owner_t = t + 1 - core
    is_owner = core == 1
    no_owner = core == 0

    barrier = pltpu.get_barrier_semaphore()

    def greet(kv, tp):
        pl.semaphore_signal(barrier, inc=1, device_id=(kv, tp), device_id_type=MESH)

    for peer in kv_peers:
        greet(peer, owner_t)

    @pl.when(is_owner)
    def _():
        for peer in kv_peers:
            greet(peer, t - 1)

    for peer in tp_peers:
        greet(k, peer)

    for n, (name, (src, dst)) in enumerate(sources.items()):
        loads[name] = pltpu.make_async_copy(src, dst, in_sem.at[n])
        loads[name].start()

    def send(src, dst, sent, received, kv, tp):
        pltpu.make_async_remote_copy(
            src_ref=src,
            dst_ref=dst,
            send_sem=sent,
            recv_sem=received,
            device_id=(kv, tp),
            device_id_type=MESH,
        ).start()

    def lanes(ref, width):
        return ref if width is None else ref.at[:, pl.ds(0, width)]

    def to_owner(phase, src, dst, peer, width=None):
        send(
            lanes(src.at[peer], width),
            lanes(dst.at[core, k], width),
            send_sem.at[phase, 0],
            recv_sem.at[phase, core],
            peer,
            owner_t,
        )

    def own_to_owner(phase, src, dst, width=None):
        @pl.when(no_owner)
        def _():
            to_owner(phase, src, dst, k, width)

        @pl.when(is_owner)
        def _():
            dst[1, pl.ds(k, 1)] = src[pl.ds(k, 1)]

    def to_members(phase, src, dst, group, width=None):
        peers = kv_peers if group else kv_peers + [k]
        for peer in peers:
            send(
                lanes(src.at[group], width),
                lanes(dst.at[k], width),
                send_sem.at[phase, group],
                recv_sem.at[phase, 0],
                peer,
                t - 1 + group,
            )

    def to_tp(phase, src, dst):
        for peer in tp_peers:
            send(src, dst.at[t], send_sem.at[phase, 0], recv_sem.at[phase, 0], k, peer)

    def wait_bytes(ref, sem):
        pltpu.make_async_copy(ref, ref, sem).wait()

    def arrived_at_owner(phase, dst, group, width=None):
        count = KV - group
        some = dst.at[group, pl.ds(0, count)]
        if width is not None:
            some = dst.at[group, pl.ds(0, count), :, pl.ds(0, width)]
        with jax.named_scope("own%d_%d" % (phase, group)):
            wait_bytes(some, recv_sem.at[phase, group])

    def arrived_at_member(phase, dst):
        for group, role in ((0, no_owner), (1, is_owner)):

            @pl.when(role)
            def _():
                with jax.named_scope("recv%d" % phase):
                    wait_bytes(dst.at[pl.ds(0, KV - group)], recv_sem.at[phase, 0])

    def arrived_tp(phase, dst):
        with jax.named_scope("recv%d" % phase):
            wait_bytes(dst.at[pl.ds(0, TP - 1)], recv_sem.at[phase, 0])

    for name in ("tok", "mix"):
        loads[name].wait()
    for s in range(SEQS):
        xs[NEW * s : NEW * s + NEW, :] = tok[s].astype(F32)
    x = xs[...]
    scaled = (x * mix[...]).astype(BF16)
    est[...] = jnp.broadcast_to(jnp.sum(x * x, axis=1, keepdims=True), (ROWS, 128))
    loads["wf"].wait()
    est[:, 0:16] = lax.dot_general(
        scaled, wf[...], (((1,), (1,)), ((), ())), preferred_element_type=F32
    )
    lane64 = lax.broadcasted_iota(jnp.int32, (ROWS, 128), 1)
    bias_all = jnp.where(lax.rem(lane64, 2) == 0, bias_ref[0], bias_ref[1])
    high = bias_all.astype(BF16).astype(F32)
    middle_part = (bias_all - high).astype(BF16).astype(F32)
    low = bias_all - high - middle_part
    parts = jnp.where(lane64 < 18, high, jnp.where(lane64 < 20, middle_part, low))
    est[...] = jnp.where((lane64 >= 16) & (lane64 < 22), parts, est[...])
    for n, (name, w) in enumerate((("wq", wq), ("wk", wk), ("wv", wv))):
        loads[name].wait()
        part = jnp.dot(scaled, w[...], preferred_element_type=F32)
        for s in range(SEQS):
            for h in range(HEADS):
                send_a[2 * s + h, :, HD * n : HD * n + HD] = part[
                    NEW * s : NEW * s + NEW, HD * h : HD * h + HD
                ].astype(BF16)
    for s in range(SEQS):
        piece = est[NEW * s : NEW * s + NEW, :].astype(BF16)
        for h in range(HEADS):
            send_a[2 * s + h, :, 3 * HD : 4 * HD] = piece
    with jax.named_scope("barrier"):
        pl.semaphore_wait(barrier, KV - 1 + TP - 1 + (KV - 1) * core)
    for peer in kv_peers:
        to_owner(0, send_a, recv_a, peer)
    own_to_owner(0, send_a, recv_a)

    qblk[...] = jnp.zeros(qblk.shape, F32)
    for name in ("kc", "vc", "cg"):
        loads[name].wait()
    score_scale = HD**-0.5
    position = k * POS + lax.broadcasted_iota(jnp.int32, (8, POS), 1)
    row8 = lax.broadcasted_iota(jnp.int32, (8, POS), 0)
    lane8 = lax.broadcasted_iota(jnp.int32, (8, 128), 1)
    for s in range(SEQS):
        length = lengths_ref[s]
        both = cg[s]
        cum = jnp.where(row8 < NEW, both[0:1, :], both[1:2, :])
        bias[s] = jnp.where(position < length, -cum, NEG_FILL)
        at_last = jnp.sum(jnp.where(position == length - 1, cum, 0.0), axis=1, keepdims=True)
        last[s] = jnp.broadcast_to(at_last, (8, 128))
    for s in range(SEQS):
        kt[s] = kc[s].T

    lane = lax.broadcasted_iota(jnp.int32, (NEW, 128), 1)

    @pl.when(is_owner)
    def _():
        for group in (1, 0):
            arrived_at_owner(0, recv_a, group)
            total = recv_a[group, 0].astype(F32)
            own_bias = total[:, 3 * HD :]
            for j in range(1, KV):
                total = total + recv_a[group, j].astype(F32)
            inv_norm = lax.rsqrt(total[:, 4 * HD - 1 : 4 * HD] / D + EPSILON)
            query = (inv_norm * total[:, 0:HD]).astype(BF16)
            send_q[group] = query
            to_members(1, send_q, recv_q, group)
            if group:
                recv_q[pl.ds(k, 1)] = query[None]
            forget_lane = 2 * (t - 1 + group) + head
            forget_sum = jnp.sum(
                jnp.where(lane == forget_lane, total[:, 3 * HD :], 0.0), axis=1, keepdims=True
            )
            of_head = (lane >= 16) & (lane < 22) & (lax.rem(lane, 2) == head)
            gate_bias = jnp.sum(jnp.where(of_head, own_bias, 0.0), axis=1, keepdims=True)
            gate_in = inv_norm * forget_sum + gate_bias
            log_forget = jnp.minimum(gate_in, 0.0) - jnp.log1p(jnp.exp(-jnp.abs(gate_in)))
            state[group, :, 0:HD] = query.astype(F32)
            for n in (1, 2):
                state[group, :, HD * n : HD * n + HD] = (
                    (inv_norm * total[:, HD * n : HD * n + HD]).astype(BF16).astype(F32)
                )
            state[group, :, 3 * HD :] = jnp.broadcast_to(log_forget, (NEW, 128))

    arrived_at_member(1, recv_q)
    for s in range(SEQS):
        for h in range(HEADS):
            qblk[s, NEW * h : NEW * h + NEW, HD * h : HD * h + HD] = recv_q[2 * s + h].astype(F32)
    for dz in (4, 5, 3, 6, 2, 7, 1, 0):
        z_peer = lax.rem(z + dz, ZS)
        for s in (2 * z_peer, 2 * z_peer + 1):
            scores = jnp.dot(qblk[s].astype(BF16), kt[s], preferred_element_type=F32)
            scores = scores * score_scale + bias[s]
            peak = jnp.maximum(jnp.max(scores, axis=1, keepdims=True), PEAK_FLOOR)
            weights = jnp.exp(scores - peak)
            block_total = jnp.sum(weights, axis=1, keepdims=True)
            block_sum = jnp.dot(weights.astype(BF16), vc[s], preferred_element_type=F32)
            stats = jnp.where(lane8 == 0, peak, jnp.where(lane8 == 1, block_total, last[s]))
            for h in range(HEADS):
                lines = slice(NEW * h, NEW * h + NEW)
                send_b[2 * s + h, :, 0:HD] = block_sum[lines, HD * h : HD * h + HD]
                send_b[2 * s + h, :, HD:] = stats[lines]
        for dy in (2, 1, 3, 0):
            if dz or dy:
                to_owner(2, send_b, recv_b, z_peer * YS + lax.rem(y + dy, YS))
    own_to_owner(2, send_b, recv_b)

    token = lax.broadcasted_iota(jnp.int32, (NEW, 1), 0)

    @pl.when(is_owner)
    def _():
        for group in (1, 0):
            arrived_at_owner(2, recv_b, group)
            past_peak = recv_b[group, 0, :, HD : HD + 1]
            for j in range(1, KV):
                past_peak = jnp.maximum(past_peak, recv_b[group, j, :, HD : HD + 1])
            past_total = jnp.zeros((NEW, 1), F32)
            last_cum = jnp.zeros((NEW, 1), F32)
            past_sum = jnp.zeros((NEW, HD), F32)
            for j in range(KV):
                stats = recv_b[group, j, :, HD:]
                factor = jnp.exp(stats[:, 0:1] - past_peak)
                past_total = past_total + stats[:, 1:2] * factor
                last_cum = last_cum + stats[:, 2:3]
                past_sum = past_sum + recv_b[group, j, :, 0:HD] * factor
            query_wide = state[group, :, 0:HD]
            key_new = state[group, :, HD : 2 * HD]
            value_new = state[group, :, 2 * HD : 3 * HD]
            log_forget = state[group, :, 3 * HD : 3 * HD + 1]
            key_cum = last_cum[0:1, :]
            own_scores = []
            for i in range(NEW):
                key_cum = key_cum + log_forget[i : i + 1, :]
                dots = jnp.sum(query_wide * key_new[i : i + 1, :], axis=1, keepdims=True)
                own_scores.append(jnp.where(token >= i, dots * score_scale - key_cum, NEG_FILL))
            peak_score = past_peak
            for score in own_scores:
                peak_score = jnp.maximum(peak_score, score)
            past_factor = jnp.exp(past_peak - peak_score)
            numerator = past_sum * past_factor
            denominator = past_total * past_factor
            for i, score in enumerate(own_scores):
                weight = jnp.where(token >= i, jnp.exp(score - peak_score), 0.0)
                numerator = numerator + weight.astype(BF16).astype(F32) * value_new[i : i + 1, :]
                denominator = denominator + weight
            attended = (numerator / denominator).astype(BF16)
            send_t[group] = attended
            to_members(3, send_t, recv_t, group)
            if group:
                recv_t[pl.ds(k, 1)] = attended[None]

    loads["wo"].wait()
    arrived_at_member(3, recv_t)
    for s in range(SEQS):
        for h in range(HEADS):
            att[NEW * s : NEW * s + NEW, HD * h : HD * h + HD] = recv_t[2 * s + h].astype(F32)

    send_c[0] = jnp.dot(att[...].astype(BF16), wo[...], preferred_element_type=F32).astype(BF16)
    to_tp(4, send_c.at[0], recv_c)
    recv_c[pl.ds(t, 1)] = send_c[...]
    for name in ("mlp", "wg", "wu"):
        loads[name].wait()
    arrived_tp(4, recv_c)
    attn_out = recv_c[0].astype(F32)
    for j in range(1, TP):
        attn_out = attn_out + recv_c[j].astype(F32)
    middle = (xs[...] + attn_out).astype(BF16).astype(F32)
    xs[...] = middle
    scaled2 = (middle * mlp[...]).astype(BF16)
    squares = jnp.broadcast_to(jnp.sum(middle * middle, axis=1, keepdims=True), (ROWS, 128))
    rough = squares.astype(BF16).astype(F32)
    est[...] = jnp.where(lane64 < 64, rough, squares - rough)

    for s in range(SEQS):
        piece = est[NEW * s : NEW * s + NEW, :].astype(BF16)
        for half in range(2):
            send_e[2 * s + half, :, 0:128] = piece

    def partial_products(dst, at, begin, width, half):
        for n, w in enumerate((wg, wu)):
            part = jnp.dot(scaled2, w[:, begin : begin + width], preferred_element_type=F32)
            for s in range(SEQS):
                dst[2 * s + half, :, at + width * n : at + width * n + width] = part[
                    NEW * s : NEW * s + NEW
                ].astype(BF16)

    for half in range(2):
        partial_products(send_e, 128, CUT * half, FIRST, half)
    for peer in kv_peers:
        to_owner(5, send_e, recv_e, peer)
    own_to_owner(5, send_e, recv_e)
    for half in range(2):
        partial_products(send_l, 0, CUT * half + FIRST, LATE[half] // 2, half)
    for dz, dy in OFFSETS:
        peer = lax.rem(z + dz, ZS) * YS + lax.rem(y + dy, YS)
        half = lax.rem(y + dy, 2)
        for h in range(2):

            @pl.when(half == h)
            def _():
                to_owner(8, send_l, recv_l, peer, LATE[h])

    for h in range(2):

        @pl.when(head == h)
        def _():
            own_to_owner(8, send_l, recv_l, LATE[h])

    def hidden_of(gate, up, inv_norm2):
        gate = inv_norm2 * gate
        return (gate * jax.nn.sigmoid(gate) * (inv_norm2 * up)).astype(BF16)

    @pl.when(is_owner)
    def _():
        for group in (1, 0):
            arrived_at_owner(5, recv_e, group)
            total = recv_e[group, 0].astype(F32)
            for j in range(1, KV):
                total = total + recv_e[group, j].astype(F32)
            inv_norm2 = lax.rsqrt((total[:, 0:1] + total[:, 127:128]) / D + EPSILON)
            hidden = hidden_of(total[:, 128 : 128 + FIRST], total[:, 128 + FIRST :], inv_norm2)
            send_h[group] = hidden
            to_members(6, send_h, recv_h, group)
            if group:
                recv_h[pl.ds(k, 1)] = hidden[None]
            state[group, :, 0:HD] = jnp.broadcast_to(inv_norm2, (NEW, HD))
        for h in range(2):

            @pl.when(head == h)
            def _():
                width = LATE[h]
                for group in (1, 0):
                    arrived_at_owner(8, recv_l, group, width)
                    total = recv_l[group, 0, :, 0:width].astype(F32)
                    for j in range(1, KV):
                        total = total + recv_l[group, j, :, 0:width].astype(F32)
                    hidden = hidden_of(
                        total[:, 0 : width // 2], total[:, width // 2 :], state[group, :, 0:1]
                    )
                    send_m[group, :, 0 : width // 2] = hidden
                    to_members(9, send_m, recv_m, group, width // 2)
                    if group:
                        recv_m[pl.ds(k, 1), :, 0 : width // 2] = hidden[None]

    loads["wd"].wait()
    arrived_at_member(6, recv_h)
    for s in range(SEQS):
        for h in range(2):
            hid[NEW * s : NEW * s + NEW, CUT * h : CUT * h + FIRST] = recv_h[2 * s + h].astype(F32)

    def by_role(enough, sem, name):
        for role, buffer in zip(
            (no_owner, is_owner & (head == 0), is_owner & (head == 1)), enough, strict=True
        ):

            @pl.when(role)
            def _():
                with jax.named_scope(name):
                    wait_bytes(buffer, sem)

    by_role(
        (recv_a.at[0, pl.ds(0, 20)], recv_e.at[0, pl.ds(0, 11)], recv_l.at[0, pl.ds(0, 13)]),
        recv_sem.at[9, 0],
        "recv9",
    )
    for s in range(SEQS):
        for h in range(2):
            begin, width = CUT * h + FIRST, LATE[h] // 2
            hid[NEW * s : NEW * s + NEW, begin : begin + width] = recv_m[
                2 * s + h, :, 0:width
            ].astype(F32)

    send_f[0] = jnp.dot(hid[...].astype(BF16), wd[...], preferred_element_type=F32).astype(BF16)
    to_tp(7, send_f.at[0], recv_f)
    recv_f[pl.ds(t, 1)] = send_f[...]
    arrived_tp(7, recv_f)
    mixed = recv_f[0].astype(F32)
    for j in range(1, TP):
        mixed = mixed + recv_f[j].astype(F32)
    out_ref[...] = (xs[...] + mixed).astype(BF16)

    for phase, buffer in ((4, recv_c), (7, recv_f)):
        wait_bytes(buffer.at[pl.ds(0, TP - 1)], send_sem.at[phase, 0])
    for group, role in ((0, no_owner), (1, is_owner)):

        @pl.when(role)
        def _():
            for phase, buffer in ((0, recv_a), (2, recv_b), (5, recv_e)):
                wait_bytes(buffer.at[0, pl.ds(0, KV - group)], send_sem.at[phase, 0])

    by_role(
        (recv_a.at[:, pl.ds(0, 20)], recv_e.at[0, pl.ds(0, 22)], recv_l.at[0, pl.ds(0, 26)]),
        send_sem.at[8, 0],
        "sent8",
    )

    @pl.when(is_owner)
    def _():
        for group in range(2):
            for phase, buffer in ((1, recv_q), (3, recv_t), (6, recv_h)):
                wait_bytes(buffer.at[pl.ds(0, KV - group)], send_sem.at[phase, group])
        for h in range(2):

            @pl.when(head == h)
            def _():
                for group in range(2):
                    some = recv_m.at[pl.ds(0, KV - group), :, pl.ds(0, LATE[h] // 2)]
                    wait_bytes(some, send_sem.at[9, group])


def on_device(
    tokens,
    mix_gain,
    w_query,
    w_key,
    w_value,
    w_forget,
    forget_bias,
    key_cache,
    value_cache,
    cum_gate,
    lengths,
    w_out,
    mlp_gain,
    w_gate,
    w_up,
    w_down,
):
    in_vmem = [
        tokens,
        mix_gain.reshape(1, WIDTH),
        w_query,
        w_key,
        w_value,
        w_forget.T,
        key_cache,
        value_cache,
        cum_gate,
        w_out,
        mlp_gain.reshape(1, WIDTH),
        w_gate,
        w_up,
        w_down,
    ]
    shapes = [pltpu.VMEM(a.shape, a.dtype) for a in in_vmem]
    shapes[5] = pltpu.VMEM((16, WIDTH), BF16)
    out = pl.pallas_call(
        kernel,
        out_shape=jax.ShapeDtypeStruct((ROWS, WIDTH), BF16),
        in_specs=[pl.BlockSpec(memory_space=pltpu.SMEM)] * 2
        + [pl.BlockSpec(memory_space=pltpu.HBM)] * len(in_vmem),
        out_specs=pl.BlockSpec(memory_space=pltpu.VMEM),
        scratch_shapes=shapes
        + [
            pltpu.VMEM((ROWS, WIDTH), F32),
            pltpu.VMEM((ROWS, 128), F32),
            pltpu.VMEM((SEQS, 8, 2 * HD), F32),
            pltpu.VMEM((SEQS, 2*HD, POS), BF16),
            pltpu.VMEM((SEQS, 8, POS), F32),
            pltpu.VMEM((SEQS, 8, 128), F32),
            pltpu.VMEM((ROWS, 2 * HD), F32),
            pltpu.VMEM((ROWS, FF), F32),
            pltpu.VMEM((2, NEW, 4 * HD), F32),
            pltpu.VMEM((KV, NEW, 4 * HD), BF16),
            pltpu.VMEM((2, KV, NEW, 4 * HD), BF16),
            pltpu.VMEM((2, NEW, HD), BF16),
            pltpu.VMEM((KV, NEW, HD), BF16),
            pltpu.VMEM((KV, NEW, 2 * HD), F32),
            pltpu.VMEM((2, KV, NEW, 2 * HD), F32),
            pltpu.VMEM((2, NEW, HD), BF16),
            pltpu.VMEM((KV, NEW, HD), BF16),
            pltpu.VMEM((1, ROWS, WIDTH), BF16),
            pltpu.VMEM((TP, ROWS, WIDTH), BF16),
            pltpu.VMEM((KV, NEW, EARLY), BF16),
            pltpu.VMEM((2, KV, NEW, EARLY), BF16),
            pltpu.VMEM((KV, NEW, LATE[0]), BF16),
            pltpu.VMEM((2, KV, NEW, LATE[0]), BF16),
            pltpu.VMEM((2, NEW, FIRST), BF16),
            pltpu.VMEM((KV, NEW, FIRST), BF16),
            pltpu.VMEM((2, NEW, LATE[0] // 2), BF16),
            pltpu.VMEM((KV, NEW, LATE[0] // 2), BF16),
            pltpu.VMEM((1, ROWS, WIDTH), BF16),
            pltpu.VMEM((TP, ROWS, WIDTH), BF16),
            pltpu.SemaphoreType.DMA((len(in_vmem),)),
            pltpu.SemaphoreType.DMA((10, 2)),
            pltpu.SemaphoreType.DMA((10, 2)),
        ],
        compiler_params=pltpu.CompilerParams(
            collective_id=0, has_side_effects=True, vmem_limit_bytes=67043328
        ),
    )(lengths, forget_bias, *in_vmem)
    return out.reshape(SEQS, NEW, WIDTH)


def solution(mesh):
    return jax.shard_map(
        on_device,
        mesh=mesh,
        in_specs=(
            P(None, None, "kv"),
            P("kv"),
            P("kv", "tp"),
            P("kv", "tp"),
            P("kv", "tp"),
            P(),
            P("tp"),
            P(None, "kv", "tp"),
            P(None, "kv", "tp"),
            P(None, "tp", "kv"),
            P(),
            P("tp", "kv"),
            P("kv"),
            P("kv", "tp"),
            P("kv", "tp"),
            P("tp", "kv"),
        ),
        out_specs=P(None, None, "kv"),
        check_vma=False,
    )
```

time: 67.8 us -> 64.5 us (0.951)
  Pallas kernels: 66.2 us -> 62.8 us
    pallas_call x1, Pallas kernels: 66.2 us -> 62.8 us  [on_device(): pl.pallas_call(kernel, out_shape=jax.ShapeDtypeStruct((ROWS, WIDTH), BF16...]
where the time goes in v3:
time: 64.5 us; the launch traced here: 64.2 us
  Pallas kernels  62.8 us (97%)
  local copies, waits for them, and re-layouts  1.33 us (2%)
    pallas_call x1, Pallas kernels, on_device(): pl.pallas_call(kernel, out_shape=jax.ShapeDtypeStruct((ROWS, WIDTH), BF16...  62.8 us
    unnamed x1, local copies, waits for them, and re-layouts  1.33 us

profile of v3, /device:TPU:1, one launch (start us, length us, event | category | flops | bytes accessed | tf_op | source)
XLA Modules:
  0.0 64.2 jit_solution(4961897147114615744)
XLA Ops:
  0.0 62.8 %shard_map.154 = bf16[64,128]{1,0:T(8,128)(2,1)} custom-call(s32[16]{0:T(128)} %lengths_ref.1, f32[2]{0:T(128)} %bias_ref.1, bf16[16,4,128]{2,1,0:T(4,128)(2,1)} %tokens_hbm.1, f32[1,128]{1,0:T(1,128)} %bitcast.6, bf16[128,256]{1,0:T(8,128)(2,1)} %wq_hbm.1, bf16[128,256]{1,0:T(8,128)(2,1)} %wk_hbm.1, bf16[128,256]{1,0:T(8,128)(2,1)} %wv_hbm.1, ...), custom_call_target="tpu_custom_call" | custom-call | tf_op jit(solution)/shard_map/pallas_call | solution.py:570
  62.9 1.3 %copy.18 = bf16[16,4,128]{2,1,0:T(4,128)(2,1)} copy(bf16[16,4,128]{2,1,0:T(4,128)(2,1)} %bitcast.5) | data formatting | bytes 32768

commit v4 on v3

--- a/solution.py
+++ b/solution.py
@@ -78,6 +78,8 @@
     state,
     send_a,
     recv_a,
+    send_k,
+    recv_k,
     send_q,
     recv_q,
     send_b,
@@ -160,23 +162,23 @@
             device_id_type=MESH,
         ).start()
 
-    def lanes(ref, width):
-        return ref if width is None else ref.at[:, pl.ds(0, width)]
-
-    def to_owner(phase, src, dst, peer, width=None):
+    def lanes(ref, width, begin=0):
+        return ref if width is None else ref.at[:, pl.ds(begin, width)]
+
+    def to_owner(phase, src, dst, peer, width=None, begin=0):
         send(
-            lanes(src.at[peer], width),
-            lanes(dst.at[core, k], width),
+            lanes(src.at[peer], width, begin),
+            lanes(dst.at[core, k], width, begin),
             send_sem.at[phase, 0],
             recv_sem.at[phase, core],
             peer,
             owner_t,
         )
 
-    def own_to_owner(phase, src, dst, width=None):
+    def own_to_owner(phase, src, dst, width=None, begin=0):
         @pl.when(no_owner)
         def _():
-            to_owner(phase, src, dst, k, width)
+            to_owner(phase, src, dst, k, width, begin)
 
         @pl.when(is_owner)
         def _():
@@ -201,11 +203,11 @@
     def wait_bytes(ref, sem):
         pltpu.make_async_copy(ref, ref, sem).wait()
 
-    def arrived_at_owner(phase, dst, group, width=None):
+    def arrived_at_owner(phase, dst, group, width=None, begin=0):
         count = KV - group
         some = dst.at[group, pl.ds(0, count)]
         if width is not None:
-            some = dst.at[group, pl.ds(0, count), :, pl.ds(0, width)]
+            some = dst.at[group, pl.ds(0, count), :, pl.ds(begin, width)]
         with jax.named_scope("own%d_%d" % (phase, group)):
             wait_bytes(some, recv_sem.at[phase, group])
 
@@ -239,18 +241,20 @@
     low = bias_all - high - middle_part
     parts = jnp.where(lane64 < 18, high, jnp.where(lane64 < 20, middle_part, low))
     est[...] = jnp.where((lane64 >= 16) & (lane64 < 22), parts, est[...])
-    for n, (name, w) in enumerate((("wq", wq), ("wk", wk), ("wv", wv))):
+    def project(name, w, dst, at):
         loads[name].wait()
         part = jnp.dot(scaled, w[...], preferred_element_type=F32)
         for s in range(SEQS):
             for h in range(HEADS):
-                send_a[2 * s + h, :, HD * n : HD * n + HD] = part[
+                dst[2 * s + h, :, at : at + HD] = part[
                     NEW * s : NEW * s + NEW, HD * h : HD * h + HD
                 ].astype(BF16)
+
+    project("wq", wq, send_a, 0)
     for s in range(SEQS):
         piece = est[NEW * s : NEW * s + NEW, :].astype(BF16)
         for h in range(HEADS):
-            send_a[2 * s + h, :, 3 * HD : 4 * HD] = piece
+            send_a[2 * s + h, :, HD:] = piece
     with jax.named_scope("barrier"):
         pl.semaphore_wait(barrier, KV - 1 + TP - 1 + (KV - 1) * core)
     for peer in kv_peers:
@@ -270,9 +274,19 @@
         cum = jnp.where(row8 < NEW, both[0:1, :], both[1:2, :])
         bias[s] = jnp.where(position < length, -cum, NEG_FILL)
         at_last = jnp.sum(jnp.where(position == length - 1, cum, 0.0), axis=1, keepdims=True)
-        last[s] = jnp.broadcast_to(at_last, (8, 128))
+        high = at_last.astype(BF16).astype(F32)
+        middle_part = (at_last - high).astype(BF16).astype(F32)
+        low = at_last - high - middle_part
+        last[s] = jnp.where(
+            lane8 == 3, high, jnp.where(lane8 == 4, middle_part, jnp.where(lane8 == 5, low, 0.0))
+        )
     for s in range(SEQS):
         kt[s] = kc[s].T
+    project("wk", wk, send_k, 0)
+    project("wv", wv, send_k, HD)
+    for peer in kv_peers:
+        to_owner(10, send_k, recv_k, peer)
+    own_to_owner(10, send_k, recv_k)
 
     lane = lax.broadcasted_iota(jnp.int32, (NEW, 128), 1)
 
@@ -281,10 +295,10 @@
         for group in (1, 0):
             arrived_at_owner(0, recv_a, group)
             total = recv_a[group, 0].astype(F32)
-            own_bias = total[:, 3 * HD :]
+            own_bias = total[:, HD:]
             for j in range(1, KV):
                 total = total + recv_a[group, j].astype(F32)
-            inv_norm = lax.rsqrt(total[:, 4 * HD - 1 : 4 * HD] / D + EPSILON)
+            inv_norm = lax.rsqrt(total[:, 2 * HD - 1 : 2 * HD] / D + EPSILON)
             query = (inv_norm * total[:, 0:HD]).astype(BF16)
             send_q[group] = query
             to_members(1, send_q, recv_q, group)
@@ -292,18 +306,15 @@
                 recv_q[pl.ds(k, 1)] = query[None]
             forget_lane = 2 * (t - 1 + group) + head
             forget_sum = jnp.sum(
-                jnp.where(lane == forget_lane, total[:, 3 * HD :], 0.0), axis=1, keepdims=True
+                jnp.where(lane == forget_lane, total[:, HD:], 0.0), axis=1, keepdims=True
             )
             of_head = (lane >= 16) & (lane < 22) & (lax.rem(lane, 2) == head)
             gate_bias = jnp.sum(jnp.where(of_head, own_bias, 0.0), axis=1, keepdims=True)
             gate_in = inv_norm * forget_sum + gate_bias
             log_forget = jnp.minimum(gate_in, 0.0) - jnp.log1p(jnp.exp(-jnp.abs(gate_in)))
             state[group, :, 0:HD] = query.astype(F32)
-            for n in (1, 2):
-                state[group, :, HD * n : HD * n + HD] = (
-                    (inv_norm * total[:, HD * n : HD * n + HD]).astype(BF16).astype(F32)
-                )
-            state[group, :, 3 * HD :] = jnp.broadcast_to(log_forget, (NEW, 128))
+            state[group, :, 3 * HD : 4 * HD] = jnp.broadcast_to(log_forget, (NEW, HD))
+            state[group, :, 4 * HD :] = jnp.broadcast_to(inv_norm, (NEW, HD))
 
     arrived_at_member(1, recv_q)
     for s in range(SEQS):
@@ -315,14 +326,20 @@
             scores = jnp.dot(qblk[s].astype(BF16), kt[s], preferred_element_type=F32)
             scores = scores * score_scale + bias[s]
             peak = jnp.maximum(jnp.max(scores, axis=1, keepdims=True), PEAK_FLOOR)
+            peak = peak.astype(BF16).astype(F32)
             weights = jnp.exp(scores - peak)
             block_total = jnp.sum(weights, axis=1, keepdims=True)
             block_sum = jnp.dot(weights.astype(BF16), vc[s], preferred_element_type=F32)
-            stats = jnp.where(lane8 == 0, peak, jnp.where(lane8 == 1, block_total, last[s]))
+            high = block_total.astype(BF16).astype(F32)
+            stats = jnp.where(
+                lane8 == 0,
+                peak,
+                jnp.where(lane8 == 1, high, jnp.where(lane8 == 2, block_total - high, last[s])),
+            )
             for h in range(HEADS):
                 lines = slice(NEW * h, NEW * h + NEW)
-                send_b[2 * s + h, :, 0:HD] = block_sum[lines, HD * h : HD * h + HD]
-                send_b[2 * s + h, :, HD:] = stats[lines]
+                send_b[2 * s + h, :, 0:HD] = block_sum[lines, HD * h : HD * h + HD].astype(BF16)
+                send_b[2 * s + h, :, HD:] = stats[lines].astype(BF16)
         for dy in (2, 1, 3, 0):
             if dz or dy:
                 to_owner(2, send_b, recv_b, z_peer * YS + lax.rem(y + dy, YS))
@@ -333,19 +350,30 @@
     @pl.when(is_owner)
     def _():
         for group in (1, 0):
+            arrived_at_owner(10, recv_k, group)
+            total = recv_k[group, 0].astype(F32)
+            for j in range(1, KV):
+                total = total + recv_k[group, j].astype(F32)
+            state[group, :, HD : 3 * HD] = (
+                (state[group, :, 4 * HD : 4 * HD + 1] * total).astype(BF16).astype(F32)
+            )
+        for group in (1, 0):
             arrived_at_owner(2, recv_b, group)
-            past_peak = recv_b[group, 0, :, HD : HD + 1]
+            past_peak = recv_b[group, 0, :, HD:].astype(F32)
             for j in range(1, KV):
-                past_peak = jnp.maximum(past_peak, recv_b[group, j, :, HD : HD + 1])
-            past_total = jnp.zeros((NEW, 1), F32)
-            last_cum = jnp.zeros((NEW, 1), F32)
+                past_peak = jnp.maximum(past_peak, recv_b[group, j, :, HD:].astype(F32))
+            past_peak = past_peak[:, 0:1]
+            weighted = jnp.zeros((NEW, HD), F32)
+            gates = jnp.zeros((NEW, HD), F32)
             past_sum = jnp.zeros((NEW, HD), F32)
             for j in range(KV):
-                stats = recv_b[group, j, :, HD:]
+                stats = recv_b[group, j, :, HD:].astype(F32)
                 factor = jnp.exp(stats[:, 0:1] - past_peak)
-                past_total = past_total + stats[:, 1:2] * factor
-                last_cum = last_cum + stats[:, 2:3]
-                past_sum = past_sum + recv_b[group, j, :, 0:HD] * factor
+                weighted = weighted + stats * factor
+                gates = gates + stats
+                past_sum = past_sum + recv_b[group, j, :, 0:HD].astype(F32) * factor
+            past_total = weighted[:, 1:2] + weighted[:, 2:3]
+            last_cum = gates[:, 3:4] + gates[:, 4:5] + gates[:, 5:6]
             query_wide = state[group, :, 0:HD]
             key_new = state[group, :, HD : 2 * HD]
             value_new = state[group, :, 2 * HD : 3 * HD]
@@ -390,14 +418,16 @@
     middle = (xs[...] + attn_out).astype(BF16).astype(F32)
     xs[...] = middle
     scaled2 = (middle * mlp[...]).astype(BF16)
-    squares = jnp.broadcast_to(jnp.sum(middle * middle, axis=1, keepdims=True), (ROWS, 128))
-    rough = squares.astype(BF16).astype(F32)
-    est[...] = jnp.where(lane64 < 64, rough, squares - rough)
-
-    for s in range(SEQS):
-        piece = est[NEW * s : NEW * s + NEW, :].astype(BF16)
-        for half in range(2):
-            send_e[2 * s + half, :, 0:128] = piece
+
+    @pl.when(is_owner)
+    def _():
+        squares = jnp.broadcast_to(jnp.sum(middle * middle, axis=1, keepdims=True), (ROWS, 128))
+        rough = squares.astype(BF16).astype(F32)
+        both_parts = jnp.where(lane64 < 64, rough, squares - rough)
+        for s in range(SEQS):
+            piece = both_parts[NEW * s : NEW * s + NEW, :].astype(BF16)
+            for half in range(2):
+                send_e[2 * s + half, :, 0:128] = piece
 
     def partial_products(dst, at, begin, width, half):
         for n, w in enumerate((wg, wu)):
@@ -409,9 +439,18 @@
 
     for half in range(2):
         partial_products(send_e, 128, CUT * half, FIRST, half)
-    for peer in kv_peers:
-        to_owner(5, send_e, recv_e, peer)
-    own_to_owner(5, send_e, recv_e)
+
+    @pl.when(is_owner)
+    def _():
+        for peer in kv_peers:
+            to_owner(5, send_e, recv_e, peer)
+
+    @pl.when(no_owner)
+    def _():
+        for peer in kv_peers:
+            to_owner(5, send_e, recv_e, peer, 2 * FIRST, 128)
+
+    own_to_owner(5, send_e, recv_e, 2 * FIRST, 128)
     for half in range(2):
         partial_products(send_l, 0, CUT * half + FIRST, LATE[half] // 2, half)
     for dz, dy in OFFSETS:
@@ -436,12 +475,18 @@
     @pl.when(is_owner)
     def _():
         for group in (1, 0):
-            arrived_at_owner(5, recv_e, group)
-            total = recv_e[group, 0].astype(F32)
+            if group:
+                arrived_at_owner(5, recv_e, 1)
+                total = recv_e[1, 0, :, 0:128].astype(F32)
+                for j in range(1, KV):
+                    total = total + recv_e[1, j, :, 0:128].astype(F32)
+                inv_norm2 = lax.rsqrt((total[:, 0:1] + total[:, 127:128]) / D + EPSILON)
+            else:
+                arrived_at_owner(5, recv_e, 0, 2 * FIRST, 128)
+            total = recv_e[group, 0, :, 128:].astype(F32)
             for j in range(1, KV):
-                total = total + recv_e[group, j].astype(F32)
-            inv_norm2 = lax.rsqrt((total[:, 0:1] + total[:, 127:128]) / D + EPSILON)
-            hidden = hidden_of(total[:, 128 : 128 + FIRST], total[:, 128 + FIRST :], inv_norm2)
+                total = total + recv_e[group, j, :, 128:].astype(F32)
+            hidden = hidden_of(total[:, 0:FIRST], total[:, FIRST:], inv_norm2)
             send_h[group] = hidden
             to_members(6, send_h, recv_h, group)
             if group:
@@ -482,7 +527,7 @@
                     wait_bytes(buffer, sem)
 
     by_role(
-        (recv_a.at[0, pl.ds(0, 20)], recv_e.at[0, pl.ds(0, 11)], recv_l.at[0, pl.ds(0, 13)]),
+        (kt.at[0, pl.ds(0, 80)], recv_e.at[0, pl.ds(0, 11)], recv_l.at[0, pl.ds(0, 13)]),
         recv_sem.at[9, 0],
         "recv9",
     )
@@ -508,11 +553,14 @@
 
         @pl.when(role)
         def _():
-            for phase, buffer in ((0, recv_a), (2, recv_b), (5, recv_e)):
+            for phase, buffer in ((0, recv_a), (2, recv_b), (10, recv_k)):
                 wait_bytes(buffer.at[0, pl.ds(0, KV - group)], send_sem.at[phase, 0])
+            first = 128 * (1 - group)
+            some = recv_e.at[0, pl.ds(0, KV - group), :, pl.ds(first, EARLY - first)]
+            wait_bytes(some, send_sem.at[5, 0])
 
     by_role(
-        (recv_a.at[:, pl.ds(0, 20)], recv_e.at[0, pl.ds(0, 22)], recv_l.at[0, pl.ds(0, 26)]),
+        (kt.at[0, pl.ds(0, 160)], recv_e.at[0, pl.ds(0, 22)], recv_l.at[0, pl.ds(0, 26)]),
         send_sem.at[8, 0],
         "sent8",
     )
@@ -583,13 +631,15 @@
             pltpu.VMEM((SEQS, 8, 128), F32),
             pltpu.VMEM((ROWS, 2 * HD), F32),
             pltpu.VMEM((ROWS, FF), F32),
-            pltpu.VMEM((2, NEW, 4 * HD), F32),
-            pltpu.VMEM((KV, NEW, 4 * HD), BF16),
-            pltpu.VMEM((2, KV, NEW, 4 * HD), BF16),
+            pltpu.VMEM((2, NEW, 5 * HD), F32),
+            pltpu.VMEM((KV, NEW, 2 * HD), BF16),
+            pltpu.VMEM((2, KV, NEW, 2 * HD), BF16),
+            pltpu.VMEM((KV, NEW, 2 * HD), BF16),
+            pltpu.VMEM((2, KV, NEW, 2 * HD), BF16),
             pltpu.VMEM((2, NEW, HD), BF16),
             pltpu.VMEM((KV, NEW, HD), BF16),
-            pltpu.VMEM((KV, NEW, 2 * HD), F32),
-            pltpu.VMEM((2, KV, NEW, 2 * HD), F32),
+            pltpu.VMEM((KV, NEW, 2 * HD), BF16),
+            pltpu.VMEM((2, KV, NEW, 2 * HD), BF16),
             pltpu.VMEM((2, NEW, HD), BF16),
             pltpu.VMEM((KV, NEW, HD), BF16),
             pltpu.VMEM((1, ROWS, WIDTH), BF16),
@@ -605,8 +655,8 @@
             pltpu.VMEM((1, ROWS, WIDTH), BF16),
             pltpu.VMEM((TP, ROWS, WIDTH), BF16),
             pltpu.SemaphoreType.DMA((len(in_vmem),)),
-            pltpu.SemaphoreType.DMA((10, 2)),
-            pltpu.SemaphoreType.DMA((10, 2)),
+            pltpu.SemaphoreType.DMA((11, 2)),
+            pltpu.SemaphoreType.DMA((11, 2)),
         ],
         compiler_params=pltpu.CompilerParams(
             collective_id=0, has_side_effects=True, vmem_limit_bytes=67043328

time: 64.5 us -> 63.5 us (0.984)
  Pallas kernels: 62.8 us -> 61.8 us
    pallas_call x1, Pallas kernels: 62.8 us -> 61.8 us  [on_device(): pl.pallas_call(kernel, out_shape=jax.ShapeDtypeStruct((ROWS, WIDTH), BF16...]
where the time goes in v4:
time: 63.5 us; the launch traced here: 63.2 us
  Pallas kernels  61.8 us (97%)
  local copies, waits for them, and re-layouts  1.33 us (2%)
    pallas_call x1, Pallas kernels, on_device(): pl.pallas_call(kernel, out_shape=jax.ShapeDtypeStruct((ROWS, WIDTH), BF16...  61.8 us
    unnamed x1, local copies, waits for them, and re-layouts  1.33 us

profile of v4, /device:TPU:1, one launch (start us, length us, event | category | flops | bytes accessed | tf_op | source)
XLA Modules:
  0.0 63.2 jit_solution(8564182589752901567)
XLA Ops:
  0.0 61.8 %shard_map.154 = bf16[64,128]{1,0:T(8,128)(2,1)} custom-call(s32[16]{0:T(128)} %lengths_ref.1, f32[2]{0:T(128)} %bias_ref.1, bf16[16,4,128]{2,1,0:T(4,128)(2,1)} %tokens_hbm.1, f32[1,128]{1,0:T(1,128)} %bitcast.6, bf16[128,256]{1,0:T(8,128)(2,1)} %wq_hbm.1, bf16[128,256]{1,0:T(8,128)(2,1)} %wk_hbm.1, bf16[128,256]{1,0:T(8,128)(2,1)} %wv_hbm.1, ...), custom_call_target="tpu_custom_call" | custom-call | tf_op jit(solution)/shard_map/pallas_call | solution.py:618
  61.9 1.3 %copy.18 = bf16[16,4,128]{2,1,0:T(4,128)(2,1)} copy(bf16[16,4,128]{2,1,0:T(4,128)(2,1)} %bitcast.5) | data formatting | bytes 32768

commit v5 on v4

--- a/solution.py
+++ b/solution.py
@@ -18,7 +18,7 @@
 POS = 512
 FF = 1408
 CUT = 768
-FIRST = 384
+FIRST = 512
 EARLY = 128 + 2 * FIRST
 LATE = (2 * (CUT - FIRST), 2 * (FF - CUT - FIRST))
 KV = 32
@@ -36,8 +36,8 @@
 
 
 def kernel(
-    lengths_ref,
-    bias_ref,
+    lengths_hbm,
+    bias_hbm,
     tokens_hbm,
     mix_hbm,
     wq_hbm,
@@ -53,6 +53,8 @@
     wu_hbm,
     wd_hbm,
     out_ref,
+    lengths_ref,
+    bias_ref,
     tok,
     mix,
     wq,
@@ -76,6 +78,7 @@
     att,
     hid,
     state,
+    blocks,
     send_a,
     recv_a,
     send_k,
@@ -112,10 +115,12 @@
     sources = dict(
         tok=(tokens_hbm, tok),
         mix=(mix_hbm, mix),
+        bias=(bias_hbm, bias_ref),
         wq=(wq_hbm, wq),
+        wf=(wf_hbm.at[:, pl.ds(pl.multiple_of(k * WIDTH, WIDTH), WIDTH)], wf),
+        lengths=(lengths_hbm, lengths_ref),
         wk=(wk_hbm, wk),
         wv=(wv_hbm, wv),
-        wf=(wf_hbm.at[:, pl.ds(pl.multiple_of(k * WIDTH, WIDTH), WIDTH)], wf),
         kc=(kc_hbm, kc),
         vc=(vc_hbm, vc),
         cg=(cg_hbm, cg),
@@ -234,6 +239,7 @@
     est[:, 0:16] = lax.dot_general(
         scaled, wf[...], (((1,), (1,)), ((), ())), preferred_element_type=F32
     )
+    loads["bias"].wait()
     lane64 = lax.broadcasted_iota(jnp.int32, (ROWS, 128), 1)
     bias_all = jnp.where(lax.rem(lane64, 2) == 0, bias_ref[0], bias_ref[1])
     high = bias_all.astype(BF16).astype(F32)
@@ -262,7 +268,7 @@
     own_to_owner(0, send_a, recv_a)
 
     qblk[...] = jnp.zeros(qblk.shape, F32)
-    for name in ("kc", "vc", "cg"):
+    for name in ("kc", "vc", "cg", "lengths"):
         loads[name].wait()
     score_scale = HD**-0.5
     position = k * POS + lax.broadcasted_iota(jnp.int32, (8, POS), 1)
@@ -516,6 +522,12 @@
         for h in range(2):
             hid[NEW * s : NEW * s + NEW, CUT * h : CUT * h + FIRST] = recv_h[2 * s + h].astype(F32)
 
+    def all_slabs(counts):
+        together = 16 * sum(counts)
+        return tuple(
+            blocks.at[pl.ds(0, n)] for n in (together, together - counts[0], together - counts[1])
+        )
+
     def by_role(enough, sem, name):
         for role, buffer in zip(
             (no_owner, is_owner & (head == 0), is_owner & (head == 1)), enough, strict=True
@@ -527,7 +539,7 @@
                     wait_bytes(buffer, sem)
 
     by_role(
-        (kt.at[0, pl.ds(0, 80)], recv_e.at[0, pl.ds(0, 11)], recv_l.at[0, pl.ds(0, 13)]),
+        all_slabs([width // 256 for width in LATE]),
         recv_sem.at[9, 0],
         "recv9",
     )
@@ -560,7 +572,7 @@
             wait_bytes(some, send_sem.at[5, 0])
 
     by_role(
-        (kt.at[0, pl.ds(0, 160)], recv_e.at[0, pl.ds(0, 22)], recv_l.at[0, pl.ds(0, 26)]),
+        all_slabs([width // 128 for width in LATE]),
         send_sem.at[8, 0],
         "sent8",
     )
@@ -617,11 +629,14 @@
     shapes[5] = pltpu.VMEM((16, WIDTH), BF16)
     out = pl.pallas_call(
         kernel,
-        out_shape=jax.ShapeDtypeStruct((ROWS, WIDTH), BF16),
-        in_specs=[pl.BlockSpec(memory_space=pltpu.SMEM)] * 2
-        + [pl.BlockSpec(memory_space=pltpu.HBM)] * len(in_vmem),
+        out_shape=pltpu.VMEM((ROWS, WIDTH), BF16),
+        in_specs=[pl.BlockSpec(memory_space=pltpu.HBM)] * (2 + len(in_vmem)),
         out_specs=pl.BlockSpec(memory_space=pltpu.VMEM),
-        scratch_shapes=shapes
+        scratch_shapes=[
+            pltpu.SMEM(lengths.shape, lengths.dtype),
+            pltpu.SMEM(forget_bias.shape, forget_bias.dtype),
+        ]
+        + shapes
         + [
             pltpu.VMEM((ROWS, WIDTH), F32),
             pltpu.VMEM((ROWS, 128), F32),
@@ -632,6 +647,7 @@
             pltpu.VMEM((ROWS, 2 * HD), F32),
             pltpu.VMEM((ROWS, FF), F32),
             pltpu.VMEM((2, NEW, 5 * HD), F32),
+            pltpu.VMEM((sum(LATE) // 8, NEW, HD), BF16),
             pltpu.VMEM((KV, NEW, 2 * HD), BF16),
             pltpu.VMEM((2, KV, NEW, 2 * HD), BF16),
             pltpu.VMEM((KV, NEW, 2 * HD), BF16),
@@ -654,12 +670,12 @@
             pltpu.VMEM((KV, NEW, LATE[0] // 2), BF16),
             pltpu.VMEM((1, ROWS, WIDTH), BF16),
             pltpu.VMEM((TP, ROWS, WIDTH), BF16),
-            pltpu.SemaphoreType.DMA((len(in_vmem),)),
+            pltpu.SemaphoreType.DMA((2 + len(in_vmem),)),
             pltpu.SemaphoreType.DMA((11, 2)),
             pltpu.SemaphoreType.DMA((11, 2)),
         ],
         compiler_params=pltpu.CompilerParams(
-            collective_id=0, has_side_effects=True, vmem_limit_bytes=67043328
+            collective_id=0, has_side_effects=True, vmem_limit_bytes=67043328 - 32768
         ),
     )(lengths, forget_bias, *in_vmem)
     return out.reshape(SEQS, NEW, WIDTH)

time: 63.5 us -> 61.6 us (0.970)
  Pallas kernels: 61.8 us -> 60.8 us
  local copies, waits for them, and re-layouts: 1.33 us -> 0.61 us
    pallas_call x1, Pallas kernels: 61.8 us -> 60.8 us  [on_device(): pl.pallas_call(kernel, out_shape=pltpu.VMEM((ROWS, WIDTH), BF16), in_spec...]
    unnamed x1, local copies, waits for them, and re-layouts: 1.33 us -> 0.61 us
where the time goes in v5:
time: 61.6 us; the launch traced here: 61.4 us
  Pallas kernels  60.8 us (99%)
    pallas_call x1, Pallas kernels, on_device(): pl.pallas_call(kernel, out_shape=pltpu.VMEM((ROWS, WIDTH), BF16), in_spec...  60.8 us

profile of v5, /device:TPU:1, one launch (start us, length us, event | category | flops | bytes accessed | tf_op | source)
XLA Modules:
  0.0 61.4 jit_solution(10525436641899630004)
XLA Ops:
  0.0 60.8 %shard_map.154 = bf16[64,128]{1,0:T(8,128)(2,1)S(1)} custom-call(s32[16]{0:T(128)} %lengths_hbm.1, f32[2]{0:T(128)} %bias_hbm.1, bf16[16,4,128]{2,1,0:T(4,128)(2,1)} %tokens_hbm.1, f32[1,128]{1,0:T(1,128)} %bitcast.6, bf16[128,256]{1,0:T(8,128)(2,1)} %wq_hbm.1, bf16[128,256]{1,0:T(8,128)(2,1)} %wk_hbm.1, bf16[128,256]{1,0:T(8,128)(2,1)} %wv_hbm.1, ...), custom_call_target="tpu_custom_call" | custom-call | tf_op jit(solution)/shard_map/pallas_call | solution.py:630
  60.8 0.6 copy.18

commit v6 on v5

--- a/solution.py
+++ b/solution.py
@@ -18,7 +18,7 @@
 POS = 512
 FF = 1408
 CUT = 768
-FIRST = 512
+FIRST = 384
 EARLY = 128 + 2 * FIRST
 LATE = (2 * (CUT - FIRST), 2 * (FF - CUT - FIRST))
 KV = 32
@@ -139,6 +139,11 @@
 
     barrier = pltpu.get_barrier_semaphore()
 
+    for n, (name, (src, dst)) in enumerate(sources.items()):
+        loads[name] = pltpu.make_async_copy(src, dst, in_sem.at[n])
+    for name in list(sources)[:5]:
+        loads[name].start()
+
     def greet(kv, tp):
         pl.semaphore_signal(barrier, inc=1, device_id=(kv, tp), device_id_type=MESH)
 
@@ -153,8 +158,7 @@
     for peer in tp_peers:
         greet(k, peer)
 
-    for n, (name, (src, dst)) in enumerate(sources.items()):
-        loads[name] = pltpu.make_async_copy(src, dst, in_sem.at[n])
+    for name in list(sources)[5:]:
         loads[name].start()
 
     def send(src, dst, sent, received, kv, tp):
@@ -365,19 +369,12 @@
             )
         for group in (1, 0):
             arrived_at_owner(2, recv_b, group)
-            past_peak = recv_b[group, 0, :, HD:].astype(F32)
-            for j in range(1, KV):
-                past_peak = jnp.maximum(past_peak, recv_b[group, j, :, HD:].astype(F32))
-            past_peak = past_peak[:, 0:1]
-            weighted = jnp.zeros((NEW, HD), F32)
-            gates = jnp.zeros((NEW, HD), F32)
-            past_sum = jnp.zeros((NEW, HD), F32)
-            for j in range(KV):
-                stats = recv_b[group, j, :, HD:].astype(F32)
-                factor = jnp.exp(stats[:, 0:1] - past_peak)
-                weighted = weighted + stats * factor
-                gates = gates + stats
-                past_sum = past_sum + recv_b[group, j, :, 0:HD].astype(F32) * factor
+            stats = recv_b[group, :, :, HD:].astype(F32)
+            past_peak = jnp.max(stats, axis=0)[:, 0:1]
+            factor = jnp.exp(stats[:, :, 0:1] - past_peak[None])
+            weighted = jnp.sum(stats * factor, axis=0)
+            gates = jnp.sum(stats, axis=0)
+            past_sum = jnp.sum(recv_b[group, :, :, 0:HD].astype(F32) * factor, axis=0)
             past_total = weighted[:, 1:2] + weighted[:, 2:3]
             last_cum = gates[:, 3:4] + gates[:, 4:5] + gates[:, 5:6]
             query_wide = state[group, :, 0:HD]

time: 61.6 us -> 61.3 us (level)
  no operation moved by 1% of the time
where the time goes in v6:
time: 61.3 us; the launch traced here: 61.1 us
  Pallas kernels  60.5 us (99%)
    pallas_call x1, Pallas kernels, on_device(): pl.pallas_call(kernel, out_shape=pltpu.VMEM((ROWS, WIDTH), BF16), in_spec...  60.5 us

profile of v6, /device:TPU:1, one launch (start us, length us, event | category | flops | bytes accessed | tf_op | source)
XLA Modules:
  0.0 61.1 jit_solution(16855703283427163080)
XLA Ops:
  0.0 60.5 %shard_map.154 = bf16[64,128]{1,0:T(8,128)(2,1)S(1)} custom-call(s32[16]{0:T(128)} %lengths_hbm.1, f32[2]{0:T(128)} %bias_hbm.1, bf16[16,4,128]{2,1,0:T(4,128)(2,1)} %tokens_hbm.1, f32[1,128]{1,0:T(1,128)} %bitcast.6, bf16[128,256]{1,0:T(8,128)(2,1)} %wq_hbm.1, bf16[128,256]{1,0:T(8,128)(2,1)} %wk_hbm.1, bf16[128,256]{1,0:T(8,128)(2,1)} %wv_hbm.1, ...), custom_call_target="tpu_custom_call" | custom-call | tf_op jit(solution)/shard_map/pallas_call | solution.py:627
  60.5 0.6 copy.18
